TPU v7x, 768 devices: a whole 4x8x12 slice. The times are simulated.
768 devices in a mesh: sp: 96 (over z, y), tp: 8 (over x, core).
Axes of the slice: x: 4, y: 8, z: 12, core: 2. Of those that a mesh axis runs over, the one named last changes fastest.
Arguments:
- normalized_sequence: bfloat16 [24576, 3072], P('sp', 'tp'), may hold values from -6 to 6
- probe_projection: bfloat16 [3072, 1024], P(None, 'tp'), may hold values from -0.109375 to 0.109375
- payload_array: bfloat16 [24576, 1024], P('sp', 'tp'), may hold values from -6 to 6
- onward_retain_scores: bfloat16 [24576, 1024], P('sp', 'tp'), may hold values from -5 to 5
- reverse_retain_scores: bfloat16 [24576, 1024], P('sp', 'tp'), may hold values from -5 to 5
- retention_slack: float32 [2, 1024], P(None, 'tp'), as said below
- additional_decay: float32 [2, 24576, 8], P(None, 'sp', 'tp'), may hold values from -1.38 to 0, as said below
- rescale_weights: float32 [1024], P('tp'), may hold values from 0.1 to 1.9
- result_cotangent: bfloat16 [24576, 1024], P('sp', 'tp'), may hold values from -6 to 6
Outputs:
- query_pre_grad: bfloat16 [24576, 1024], P('sp', 'tp')
- gate_fwd_grad: float32 [24576, 1024], P('sp', 'tp')
- gate_bwd_grad: float32 [24576, 1024], P('sp', 'tp')
- value_grad: bfloat16 [24576, 1024], P('sp', 'tp')
- query_weight_grad: float32 [3072, 1024], P('sp', 'tp')
Inputs may be any that keep to these rules, and one draw needn't show every extreme that they name: `retention_slack`: every entry is positive. `additional_decay`: zero except at a few positions.
All inputs are finite; a program needn't handle non-finite values.
Results may differ from a plain program's by a relative error of at most 0.025.
Values may be sent and summed in bfloat16 or wider, within the bound.
A program may use at most 64 MiB of HBM per device.

v0:
```python
import jax
import jax.numpy as jnp
from jax import lax
from jax.sharding import Mesh
from jax.sharding import PartitionSpec as P

ATTENTION_WIDTH = 128
BLOCK = 128
SP = ("sp_0", "sp_1")


epsilon = 1e-06


def nothing_yet(x, identity):
    return jax.tree.map(
        lambda a, e: jnp.broadcast_to(jnp.asarray(e, a.dtype), a.shape), x, identity
    )


def entering(x, axes, combine, identity, reverse):
    before = start = nothing_yet(x, identity)
    subtotal = x
    for axis in reversed(axes):
        peers, place = (lax.axis_size(axis), lax.axis_index(axis))
        pieces = jax.tree.map(lambda part: lax.all_gather(part, axis), subtotal)
        inside, subtotal = (start, start)
        for k in reversed(range(peers)) if reverse else range(peers):
            passed = k > place if reverse else k < place
            subtotal = combine(subtotal, jax.tree.map(lambda part: part[k], pieces))
            inside = jax.tree.map(lambda new, old: jnp.where(passed, new, old), subtotal, inside)
        before = combine(inside, before)
    return before


def own_block(parts, axes, turns):
    shape = [lax.axis_size(a) for a in axes]
    parts = parts.reshape(*shape, *parts.shape[1:])
    parts = parts.transpose(*turns, *range(len(axes), parts.ndim))
    parts = parts.reshape(-1, *parts.shape[len(axes) :])
    for k in turns:
        parts = lax.psum_scatter(parts, axes[k], scatter_dimension=0, tiled=True)
    return parts[0]


def split_up(x, dim, peers):
    shape = x.shape
    parts = x.reshape(*shape[:dim], peers, shape[dim] // peers, *shape[dim + 1 :])
    return jnp.moveaxis(parts, dim, 0)


def summed_rows(x, axes, turns, dim):
    peers = lax.axis_size(axes)
    return own_block(split_up(x, dim, peers), axes, turns)


def laid_out(parts, dim):
    parts = jnp.moveaxis(parts, 0, dim)
    shape = parts.shape
    return parts.reshape(*shape[:dim], shape[dim] * shape[dim + 1], *shape[dim + 2 :])


def sent_to_all(x, axis):
    peers = lax.axis_size(axis)
    return lax.all_to_all(jnp.broadcast_to(x[None], (peers, *x.shape)), axis, 0, 0, tiled=True)


def gathered_copies(x, axis, dim):
    return laid_out(sent_to_all(x, axis), dim)


def recurrence(queries, key_matrix, values, forget_logarithm, initial):
    length, attention_count = (queries.shape[0], queries.shape[1])
    block_count = length // BLOCK
    within_mask = jnp.tril(jnp.ones((BLOCK, BLOCK), bool))
    highest = lax.Precision.HIGHEST

    def advance(carried_state, segment):
        query_seg, key_seg, value_seg, forget_seg = segment
        running = jnp.cumsum(forget_seg, axis=0)
        query_dec = query_seg * jnp.exp(running)
        key_dec = key_seg * jnp.exp(-running)
        scores = jnp.einsum("thd,shd->hts", query_dec, key_dec, precision=highest)
        scores = jnp.where(within_mask[None], scores, 0.0)
        output = jnp.einsum("hts,she->the", scores, value_seg, precision=highest)
        output = output + jnp.einsum("thd,hde->the", query_dec, carried_state, precision=highest)
        closing = running[-1]
        carried_state = jnp.exp(closing)[:, :, None] * carried_state + jnp.einsum(
            "shd,she->hde", key_seg * jnp.exp(closing[None] - running), value_seg, precision=highest
        )
        return (carried_state, output)

    blocks = tuple(
        (
            member.reshape((block_count, BLOCK) + member.shape[1:])
            for member in (queries, key_matrix, values, forget_logarithm)
        )
    )
    final_state, outputs = lax.scan(jax.checkpoint(advance), initial, blocks)
    return outputs.reshape(length, attention_count, values.shape[2])


def retention_update(gate_input_rows, margin_row, spike_column):
    key_matrix = margin_row * jax.nn.sigmoid(-gate_input_rows)
    forget_logarithm = jnp.log1p(-key_matrix) + spike_column[:, :, None]
    return (key_matrix, forget_logarithm)


def blending_update(
    probe_before_activation,
    onward_raw_scores,
    reverse_raw_scores,
    payload_entries,
    onward_seed_memory,
    reverse_seed_memory,
    retention_slack,
    additional_decay,
    rescale_weights,
):
    length = probe_before_activation.shape[0]
    attention_count = probe_before_activation.shape[1] // ATTENTION_WIDTH

    def partition_attention(array):
        return array.reshape(length, attention_count, ATTENTION_WIDTH)

    queries = partition_attention(jax.nn.silu(probe_before_activation) * ATTENTION_WIDTH ** (-0.5))
    values = partition_attention(payload_entries)
    onward_addressing, onward_retention = retention_update(
        partition_attention(onward_raw_scores),
        retention_slack[0].reshape(attention_count, ATTENTION_WIDTH),
        additional_decay[0],
    )
    reverse_addressing, reverse_retention = retention_update(
        partition_attention(reverse_raw_scores),
        retention_slack[1].reshape(attention_count, ATTENTION_WIDTH),
        additional_decay[1],
    )
    out_fwd = recurrence(queries, onward_addressing, values, onward_retention, onward_seed_memory)
    out_bwd = jnp.flip(
        recurrence(
            jnp.flip(queries, 0),
            jnp.flip(reverse_addressing, 0),
            jnp.flip(values, 0),
            jnp.flip(reverse_retention, 0),
            reverse_seed_memory,
        ),
        0,
    )
    mixed = out_fwd + out_bwd
    normed = mixed * lax.rsqrt(jnp.mean(mixed * mixed, axis=-1, keepdims=True) + epsilon)
    normed = normed * rescale_weights.reshape(attention_count, ATTENTION_WIDTH)
    return normed.reshape(length, attention_count * ATTENTION_WIDTH)


def closing_state(
    gate_input_rows, payload_entries, carried_state, margin_row, spike_column, backward_sweep
):
    if backward_sweep:
        gate_input_rows = jnp.flip(gate_input_rows, 0)
        payload_entries = jnp.flip(payload_entries, 0)
        spike_column = jnp.flip(spike_column, 0)
    key_matrix, forget_logarithm = retention_update(gate_input_rows, margin_row, spike_column)
    running = jnp.cumsum(forget_logarithm, axis=0)
    closing = running[-1]
    summary = jnp.exp(closing)[:, :, None] * carried_state + jnp.einsum(
        "thd,the->hde",
        key_matrix * jnp.exp(closing[None] - running),
        payload_entries,
        precision=lax.Precision.HIGHEST,
    )
    return (jnp.exp(closing), summary)


def combine(earlier, later):
    return (earlier[0] * later[0], later[0][:, :, None] * earlier[1] + later[1])


def chain(elements, identity, backward_sweep):
    return entering(elements, SP, combine, identity, backward_sweep)[1]


def weight_rows(whole, query_pre_grad):
    return summed_rows(
        lax.dot_general(
            whole, query_pre_grad, (((0,), (0,)), ((), ())), preferred_element_type=jnp.float32
        ),
        SP,
        (1, 0),
        0,
    )


def on_device(
    normalized_sequence,
    probe_projection,
    payload_array,
    onward_retain_scores,
    reverse_retain_scores,
    retention_slack,
    additional_decay,
    rescale_weights,
    result_cotangent,
):
    whole = gathered_copies(normalized_sequence, "tp", 1)
    probe_before_activation = jnp.dot(
        whole, probe_projection, preferred_element_type=jnp.float32
    ).astype(jnp.bfloat16)
    length = payload_array.shape[0]
    attention_count = payload_array.shape[1] // ATTENTION_WIDTH

    def partition_attention(array):
        return array.astype(jnp.float32).reshape(length, attention_count, ATTENTION_WIDTH)

    forward_margin = retention_slack[0].reshape(attention_count, ATTENTION_WIDTH)
    backward_margin = retention_slack[1].reshape(attention_count, ATTENTION_WIDTH)
    blank_memory = jnp.zeros((attention_count, ATTENTION_WIDTH, ATTENTION_WIDTH), jnp.float32)
    identity = (jnp.ones((attention_count, ATTENTION_WIDTH), jnp.float32), blank_memory)
    decay_fwd, summary_fwd = closing_state(
        partition_attention(onward_retain_scores),
        partition_attention(payload_array),
        blank_memory,
        forward_margin,
        additional_decay[0],
        False,
    )
    decay_bwd, summary_bwd = closing_state(
        partition_attention(reverse_retain_scores),
        partition_attention(payload_array),
        blank_memory,
        backward_margin,
        additional_decay[1],
        True,
    )
    onward_seed_memory = chain((decay_fwd, summary_fwd), identity, False)
    reverse_seed_memory = chain((decay_bwd, summary_bwd), identity, True)

    def local(
        probe_raw_scores,
        onward_raw_scores,
        reverse_raw_scores,
        payload_entries,
        entry_fwd,
        entry_bwd,
    ):
        return blending_update(
            probe_raw_scores,
            onward_raw_scores,
            reverse_raw_scores,
            payload_entries,
            entry_fwd,
            entry_bwd,
            retention_slack,
            additional_decay,
            rescale_weights,
        )

    unused, pullback = jax.vjp(
        local,
        probe_before_activation.astype(jnp.float32),
        onward_retain_scores.astype(jnp.float32),
        reverse_retain_scores.astype(jnp.float32),
        payload_array.astype(jnp.float32),
        onward_seed_memory,
        reverse_seed_memory,
    )
    grad_query, grad_fwd, grad_bwd, grad_value, sense_fwd, sense_bwd = pullback(
        result_cotangent.astype(jnp.float32)
    )
    query_pre_grad = grad_query.astype(jnp.bfloat16)
    weight_grad = None
    after_fwd = chain((decay_fwd, sense_fwd), identity, True)
    after_bwd = chain((decay_bwd, sense_bwd), identity, False)

    def leaving(onward_raw_scores, reverse_raw_scores, payload_entries):
        return (
            closing_state(
                partition_attention(onward_raw_scores),
                partition_attention(payload_entries),
                onward_seed_memory,
                forward_margin,
                additional_decay[0],
                False,
            )[1],
            closing_state(
                partition_attention(reverse_raw_scores),
                partition_attention(payload_entries),
                reverse_seed_memory,
                backward_margin,
                additional_decay[1],
                True,
            )[1],
        )

    unused_end, pull_end = jax.vjp(
        leaving,
        onward_retain_scores.astype(jnp.float32),
        reverse_retain_scores.astype(jnp.float32),
        payload_array.astype(jnp.float32),
    )
    extra_fwd, extra_bwd, extra_value = pull_end((after_fwd, after_bwd))
    weight_grad = weight_rows(whole, query_pre_grad)
    return (
        query_pre_grad,
        grad_fwd + extra_fwd,
        grad_bwd + extra_bwd,
        (grad_value + extra_value).astype(jnp.bfloat16),
        weight_grad,
    )


def solution(mesh):
    torus = Mesh(mesh.devices.reshape(12, 8, mesh.shape["tp"]), ("sp_0", "sp_1", "tp"))
    return jax.shard_map(
        on_device,
        mesh=torus,
        in_specs=(
            P(SP, "tp"),
            P(None, "tp"),
            P(SP, "tp"),
            P(SP, "tp"),
            P(SP, "tp"),
            P(None, "tp"),
            P(None, SP, "tp"),
            P("tp"),
            P(SP, "tp"),
        ),
        out_specs=(P(SP, "tp"), P(SP, "tp"), P(SP, "tp"), P(SP, "tp"), P(SP, "tp")),
        check_vma=False,
    )
```

profile of v0, /device:TPU:6, one launch (start us, length us, event | category | flops | bytes accessed | tf_op | source)
XLA Modules:
  0.0 528.3 jit_solution(9755712680061517450)
XLA Ops:
  9.6 13.1 %all-to-all-start = ((bf16[8,256,384]{1,2,0:T(8,128)(2,1)}), bf16[8,256,384]{1,2,0:T(8,128)(2,1)S(1)}, u32[]{:S(2)}, u32[]{:S(2)}) async-start(bf16[8,256,384]{1,2,0:T(8,128)(2,1)} %broadcast_in_dim.145), calls=%async_computation | async-start | bytes 3145728 | tf_op jit(solution)/shard_map/all_to_all | solution.py:65
  24.3 13.3 %all_gather.73 = f32[8,1,128]{2,1,0:T(1,128)S(1)} all-gather(f32[1,1,128]{2,1,0:T(1,128)S(1)} %get-tuple-element.1133), channel_id=1, replica_groups=mesh['sp_0'=12,'sp_1'=8,'tp'=8] {'sp_1'}, dimensions={0}, use_global_device_ids=true | all-gather | bytes 4608 | tf_op jit(solution)/shard_map/all_gather | solution.py:26
  42.4 15.3 %all_gather.68 = f32[8,1,128]{2,1,0:T(1,128)S(1)} all-gather(f32[1,1,128]{2,1,0:T(1,128)S(1)} %get-tuple-element.1135), channel_id=1, replica_groups=mesh['sp_0'=12,'sp_1'=8,'tp'=8] {'sp_1'}, dimensions={0}, use_global_device_ids=true | all-gather | bytes 4608 | tf_op jit(solution)/shard_map/all_gather | solution.py:26
  61.4 25.2 %all-gather.1 = f32[1024,128]{1,0:T(8,128)S(1)} all-gather(f32[128,128]{1,0:T(8,128)S(1)} %convolution_add_fusion.4), channel_id=3, replica_groups=mesh['sp_0'=12,'sp_1'=8,'tp'=8] {'sp_1'}, dimensions={0}, use_global_device_ids=true | all-gather | bytes 589824 | tf_op jit(solution)/shard_map/all_gather | solution.py:26
  88.3 32.8 %all_gather.77 = f32[12,1,128,128]{3,2,1,0:T(8,128)} all-gather(f32[1,1,128,128]{3,2,1,0:T(8,128)S(1)} %bitcast_add_fusion.137), channel_id=1, replica_groups=mesh['sp_0'=12,'sp_1'=8,'tp'=8] {'sp_0'}, dimensions={0}, use_global_device_ids=true | all-gather | bytes 851968 | tf_op jit(solution)/shard_map/all_gather | solution.py:26
  121.1 19.9 %all_gather.74 = f32[12,1,128]{2,1,0:T(1,128)S(1)} all-gather(f32[1,1,128]{2,1,0:T(1,128)} %get-tuple-element.1206), channel_id=1, replica_groups=mesh['sp_0'=12,'sp_1'=8,'tp'=8] {'sp_0'}, dimensions={0}, use_global_device_ids=true | all-gather | bytes 6656 | tf_op jit(solution)/shard_map/all_gather | solution.py:26
  142.5 27.2 %all-gather = f32[1024,128]{1,0:T(8,128)} all-gather(f32[128,128]{1,0:T(8,128)S(1)} %convolution_add_fusion.5), channel_id=2, replica_groups=mesh['sp_0'=12,'sp_1'=8,'tp'=8] {'sp_1'}, dimensions={0}, use_global_device_ids=true | all-gather | bytes 589824 | tf_op jit(solution)/shard_map/all_gather | solution.py:26
  169.8 21.5 %all_gather.69 = f32[12,1,128]{2,1,0:T(1,128)S(1)} all-gather(f32[1,1,128]{2,1,0:T(1,128)S(1)} %copy-done.133), channel_id=1, replica_groups=mesh['sp_0'=12,'sp_1'=8,'tp'=8] {'sp_0'}, dimensions={0}, use_global_device_ids=true | all-gather | bytes 6656 | tf_op jit(solution)/shard_map/all_gather | solution.py:26
  195.8 23.9 %all_gather.72 = f32[12,1,128,128]{3,2,1,0:T(8,128)S(1)} all-gather(f32[1,1,128,128]{3,2,1,0:T(8,128)S(1)} %bitcast_add_fusion.153), channel_id=1, replica_groups=mesh['sp_0'=12,'sp_1'=8,'tp'=8] {'sp_0'}, dimensions={0}, use_global_device_ids=true | all-gather | bytes 851968 | tf_op jit(solution)/shard_map/all_gather | solution.py:26
  221.5 21.5 %all_gather.82 = f32[12,1,128]{2,1,0:T(1,128)S(1)} all-gather(f32[1,1,128]{2,1,0:T(1,128)S(1)} %copy-done.132), channel_id=1, replica_groups=mesh['sp_0'=12,'sp_1'=8,'tp'=8] {'sp_0'}, dimensions={0}, use_global_device_ids=true | all-gather | bytes 6656 | tf_op jit(solution)/shard_map/all_gather | solution.py:26
  243.0 19.9 %all_gather.78 = f32[12,1,128]{2,1,0:T(1,128)S(1)} all-gather(f32[1,1,128]{2,1,0:T(1,128)S(1)} %copy-done.131), channel_id=1, replica_groups=mesh['sp_0'=12,'sp_1'=8,'tp'=8] {'sp_0'}, dimensions={0}, use_global_device_ids=true | all-gather | bytes 6656 | tf_op jit(solution)/shard_map/all_gather | solution.py:26
  266.8 7.1 %while.79 = (s32[]{:T(128)}, f32[1,128,128]{2,1,0:T(8,128)S(1)}, f32[2,128,1,128]{3,1,0,2:T(8,128)}, f32[2,1,128,128]{3,2,1,0:T(8,128)}, f32[2,128,1,128]{3,1,2,...) while((s32[]{:T(128)}, f32[1,128,128]{2,1,0:T(8,128)S(1)}, ...), condition=%wide.region_4.5_spmd.clone, body=%wide.region_2.4_spmd.clone.sunk | while | flops 102924288 | bytes 1971309 | solution.py:99
  276.1 7.1 %while.78 = (s32[]{:T(128)}, f32[1,128,128]{2,1,0:T(8,128)S(1)}, f32[2,128,1,128]{3,1,0,2:T(8,128)}, f32[2,1,128,128]{3,2,1,0:T(8,128)}, f32[2,128,1,128]{3,1,2,...) while((s32[]{:T(128)}, f32[1,128,128]{2,1,0:T(8,128)S(1)}, ...), condition=%wide.region_9.10_spmd.clone, body=%wide.region_7.9_spmd.clone.sunk | while | flops 102924288 | bytes 1971309 | solution.py:99
  290.4 21.5 %while.81 = (s32[]{:T(128)}, f32[1,128,128]{1,2,0:T(8,128)}, f32[2,128,1,128]{3,1,2,0:T(8,128)}, f32[2,128,1,128]{3,1,2,0:T(8,128)}, f32[2,128,1,128]{1,0,3,2:T(...) while((s32[]{:T(128)}, f32[1,128,128]{1,2,0:T(8,128)}, ...), condition=%wide.region_23.24_spmd.clone, body=%wide.region_18.23_spmd.clone.sunk | while | flops 231342080 | bytes 4972727 | solution.py:99
  297.0 2.8 dynamic_update_slice.135
  308.2 2.8 dynamic_update_slice.135
  313.9 22.1 %while.80 = (s32[]{:T(128)}, f32[1,128,128]{1,2,0:T(8,128)}, f32[2,128,1,128]{3,1,2,0:T(8,128)}, f32[2,128,1,128]{3,1,2,0:T(8,128)}, f32[2,128,1,128]{1,0,3,2:T(...) while((s32[]{:T(128)}, f32[1,128,128]{1,2,0:T(8,128)}, ...), condition=%wide.region_17.18_spmd.clone, body=%wide.region_12.17_spmd.clone.sunk | while | flops 231342080 | bytes 6021359 | solution.py:99
  320.8 2.8 dynamic_update_slice.132
  332.3 2.8 dynamic_update_slice.132
  344.5 25.8 %all-gather.3 = f32[8,128,128]{2,1,0:T(8,128)S(1)} all-gather(f32[1,128,128]{2,1,0:T(8,128)S(1)} %copy.246), channel_id=5, replica_groups=mesh['sp_0'=12,'sp_1'=8,'tp'=8] {'sp_1'}, dimensions={0}, use_global_device_ids=true | all-gather | bytes 589824 | tf_op jit(solution)/shard_map/all_gather | solution.py:26
  370.5 25.9 %all_gather.85 = f32[12,1,128,128]{3,2,1,0:T(8,128)S(1)} all-gather(f32[1,1,128,128]{3,2,1,0:T(8,128)S(1)} %bitcast_add_fusion.81), channel_id=1, replica_groups=mesh['sp_0'=12,'sp_1'=8,'tp'=8] {'sp_0'}, dimensions={0}, use_global_device_ids=true | all-gather | bytes 851968 | tf_op jit(solution)/shard_map/all_gather | solution.py:26
  398.7 25.2 %all-gather.2 = f32[8,128,128]{2,1,0:T(8,128)S(1)} all-gather(f32[1,128,128]{2,1,0:T(8,128)S(1)} %copy.240), channel_id=4, replica_groups=mesh['sp_0'=12,'sp_1'=8,'tp'=8] {'sp_1'}, dimensions={0}, use_global_device_ids=true | all-gather | bytes 589824 | tf_op jit(solution)/shard_map/all_gather | solution.py:26
  424.2 23.9 %all_gather.81 = f32[12,1,128,128]{3,2,1,0:T(8,128)S(1)} all-gather(f32[1,1,128,128]{3,2,1,0:T(8,128)S(1)} %bitcast_add_fusion.121), channel_id=1, replica_groups=mesh['sp_0'=12,'sp_1'=8,'tp'=8] {'sp_0'}, dimensions={0}, use_global_device_ids=true | all-gather | bytes 851968 | tf_op jit(solution)/shard_map/all_gather | solution.py:26
  469.9 51.6 %reduce-scatter.5.cloned.1.call-done = f32[1,32,128]{2,1,0:T(8,128)} async-done(((f32[12,32,128]{2,1,0:T(8,128)}), f32[1,32,128]{2,1,0:T(8,128)}) %reduce-scatter.5.cloned.1.call-update) | async-done | bytes 16400 | tf_op jit(solution)/shard_map/reduce_scatter | solution.py:42
  (537 shorter events, 114.3 us)
Async XLA Ops:
  7.2 257.0 %copy-start = (bf16[3072,128]{1,0:T(8,128)(2,1)S(1)}, bf16[3072,128]{1,0:T(8,128)(2,1)}, u32[]{:S(2)}) copy-start(bf16[3072,128]{1,0:T(8,128)(2,1)} %param.18) | copy-start | bytes 2359300
  9.6 254.6 %all-to-all-start = ((bf16[8,256,384]{1,2,0:T(8,128)(2,1)}), bf16[8,256,384]{1,2,0:T(8,128)(2,1)S(1)}, u32[]{:S(2)}, u32[]{:S(2)}) async-start(bf16[8,256,384]{1,2,0:T(8,128)(2,1)} %broadcast_in_dim.145), calls=%async_computation | async-start | bytes 3145728 | tf_op jit(solution)/shard_map/all_to_all | solution.py:65
  22.7 446.3 %reduce-scatter.3.cloned.1.call-start = ((), (), s32[]{:S(2)}) async-start(), calls=%async_computation.3 | async-start | bytes 1769472 | tf_op jit(solution)/shard_map/reduce_scatter | solution.py:42
  38.8 102.2 %copy-start.24 = (f32[256,128]{1,0:T(8,128)}, f32[256,128]{1,0:T(8,128)S(1)}, u32[]{:S(2)}) copy-start(f32[256,128]{1,0:T(8,128)S(1)} %reverse.16) | copy-start | bytes 393220
  40.6 80.6 %copy-start.20 = (f32[128,1,2,128]{0,3,2,1:T(8,128)}, f32[128,1,2,128]{0,3,2,1:T(8,128)S(1)}, u32[]{:S(2)}) copy-start(f32[128,1,2,128]{0,3,2,1:T(8,128)S(1)} %copy.210) | copy-start | bytes 393220
  41.3 79.8 %copy-start.22 = (f32[128,2,128]{0,2,1:T(8,128)}, f32[128,2,128]{0,2,1:T(8,128)S(1)}, u32[]{:S(2)}) copy-start(f32[128,2,128]{0,2,1:T(8,128)S(1)} %broadcast.4854) | copy-start | bytes 393220
  60.1 82.4 %copy-start.10 = (f32[256,128]{1,0:T(8,128)}, f32[256,128]{1,0:T(8,128)S(1)}, u32[]{:S(2)}) copy-start(f32[256,128]{1,0:T(8,128)S(1)} %reverse.17) | copy-start | bytes 393220
  86.6 83.2 %copy-start.133 = (f32[1,1,128]{2,1,0:T(1,128)S(1)}, f32[1,1,128]{2,1,0:T(1,128)}, u32[]{:S(2)}) copy-start(f32[1,1,128]{2,1,0:T(1,128)} %get-tuple-element.1193) | copy-start | bytes 1540
  86.6 104.7 %copy-start.54 = (f32[128]{0:T(128)S(1)}, f32[128]{0:T(128)}, u32[]{:S(2)}) copy-start(f32[128]{0:T(128)} %get-tuple-element.1212) | copy-start | bytes 1540
  86.6 104.7 %copy-start.56 = (f32[128]{0:T(128)S(1)}, f32[128]{0:T(128)}, u32[]{:S(2)}) copy-start(f32[128]{0:T(128)} %get-tuple-element.1213) | copy-start | bytes 1540
  86.6 104.7 %copy-start.58 = (f32[128]{0:T(128)S(1)}, f32[128]{0:T(128)}, u32[]{:S(2)}) copy-start(f32[128]{0:T(128)} %get-tuple-element.1214) | copy-start | bytes 1540
  86.7 104.7 %copy-start.72 = (f32[128]{0:T(128)S(1)}, f32[128]{0:T(128)}, u32[]{:S(2)}) copy-start(f32[128]{0:T(128)} %get-tuple-element.1208) | copy-start | bytes 1540
  86.7 104.7 %copy-start.74 = (f32[128]{0:T(128)S(1)}, f32[128]{0:T(128)}, u32[]{:S(2)}) copy-start(f32[128]{0:T(128)} %get-tuple-element.1209) | copy-start | bytes 1540
  86.7 104.7 %copy-start.86 = (f32[128]{0:T(128)S(1)}, f32[128]{0:T(128)}, u32[]{:S(2)}) copy-start(f32[128]{0:T(128)} %get-tuple-element.1207) | copy-start | bytes 1540
  86.7 104.7 %copy-start.94 = (f32[128]{0:T(128)S(1)}, f32[128]{0:T(128)}, u32[]{:S(2)}) copy-start(f32[128]{0:T(128)} %broadcast_select_fusion.17) | copy-start | bytes 1540
  343.6 53.8 %copy-start.25 = (f32[256,128]{1,0:T(8,128)S(1)}, f32[256,128]{1,0:T(8,128)}, u32[]{:S(2)}) copy-start(f32[256,128]{1,0:T(8,128)} %copy-done.24) | copy-start | bytes 393220
  343.6 53.7 %copy-start.51 = (f32[256,1,128]{2,0,1:T(8,128)S(1)}, f32[256,1,128]{2,0,1:T(8,128)}, u32[]{:S(2)}) copy-start(f32[256,1,128]{2,0,1:T(8,128)} %copy-done.50) | copy-start | bytes 393220
  343.6 53.7 %copy-start.97 = (f32[128]{0:T(128)S(1)}, f32[128]{0:T(128)}, u32[]{:S(2)}) copy-start(f32[128]{0:T(128)} %get-tuple-element.1136) | copy-start | bytes 1540
  343.6 53.7 %copy-start.99 = (f32[128]{0:T(128)S(1)}, f32[128]{0:T(128)}, u32[]{:S(2)}) copy-start(f32[128]{0:T(128)} %get-tuple-element.1189) | copy-start | bytes 1540
  343.6 53.7 %copy-start.109 = (f32[128]{0:T(128)S(1)}, f32[128]{0:T(128)}, u32[]{:S(2)}) copy-start(f32[128]{0:T(128)} %get-tuple-element.1141) | copy-start | bytes 1540
  343.6 53.7 %copy-start.111 = (f32[128]{0:T(128)S(1)}, f32[128]{0:T(128)}, u32[]{:S(2)}) copy-start(f32[128]{0:T(128)} %get-tuple-element.1142) | copy-start | bytes 1540
  343.6 53.7 %copy-start.113 = (f32[128]{0:T(128)S(1)}, f32[128]{0:T(128)}, u32[]{:S(2)}) copy-start(f32[128]{0:T(128)} %get-tuple-element.1143) | copy-start | bytes 1540
  343.7 53.7 %copy-start.115 = (f32[128]{0:T(128)S(1)}, f32[128]{0:T(128)}, u32[]{:S(2)}) copy-start(f32[128]{0:T(128)} %get-tuple-element.1144) | copy-start | bytes 1540
  343.8 177.7 %reduce-scatter.5.cloned.1.call-start = ((), (), s32[]{:S(2)}) async-start(), calls=%async_computation.4 | async-start | bytes 212992 | tf_op jit(solution)/shard_map/reduce_scatter | solution.py:42
  (116 other events, 2576.6 us)
Sparse Core Ops, SparseCore 0:
  343.9 40.2 reduce-scatter.2
  469.2 52.2 reduce-scatter.4
where the time goes:
time: 530 us; the launch traced here: 528 us
  blocking collectives  321 us (61%)
  local copies, waits for them, and re-layouts  57.1 us (11%)
  waiting for transfers between devices  51.6 us (10%)
  other arithmetic  37.4 us (7%)
  matrix products  31.1 us (6%)
  between operations  16 us (3%)
  starting transfers between devices  13.2 us (2%)
    all_gather x14, blocking collectives, entering(): pieces = jax.tree.map(lambda part: lax.all_gather(part, axis), subtotal)  321 us
    reduce_scatter x2, waiting for transfers between devices, own_block(): parts = lax.psum_scatter(parts, axes[k], scatter_dimension=0, tiled=True)  51.6 us
    dynamic_update_slice x20, local copies, waits for them, and re-layouts, recurrence(): final_state, outputs = lax.scan(jax.checkpoint(advance), initial, blocks)  17.9 us
    all_to_all x1, starting transfers between devices, sent_to_all(): lax.all_to_all(jnp.broadcast_to(x[None], (peers, *x.shape)), axis, 0, 0,...  13.1 us
    dynamic_slice x24, local copies, waits for them, and re-layouts, recurrence(): final_state, outputs = lax.scan(jax.checkpoint(advance), initial, blocks)  12.5 us
  transfers between devices with their start and end apart: 3, of which 1 were waited for; matrix products, arithmetic and copies ran while one was open for 8% of the time, Pallas kernels for 0%

commit v1 on v0

v1 whole, which is shorter than its diff:
```python
import functools

import jax
import jax.numpy as jnp
from jax import lax
from jax.experimental import pallas as pl
from jax.experimental.pallas import tpu as pltpu
from jax.sharding import Mesh
from jax.sharding import PartitionSpec as P

WIDTH = 128
HALF = 128
NZ, NY = 12, 8
EPS = 1e-6
MESH_ID = pl.DeviceIdType.MESH
F32, BF16 = jnp.float32, jnp.bfloat16

NN = (((1,), (0,)), ((), ()))
NT = (((1,), (1,)), ((), ()))
TN = (((0,), (0,)), ((), ()))


def dot(a, b, dims):
    a, b = (p if isinstance(p, tuple) else (p,) for p in (a, b))
    total = lax.dot_general(a[0], b[0], dims, preferred_element_type=F32)
    for tail in a[1:]:
        total += lax.dot_general(tail, b[0], dims, preferred_element_type=F32)
    for tail in b[1:]:
        total += lax.dot_general(a[0], tail, dims, preferred_element_type=F32)
    return total


def pair_of(x):
    head = x.astype(BF16)
    return head, (x - head.astype(F32)).astype(BF16)


def cut(pair, *at):
    return tuple(part[at] for part in pair)


def pieces(x, count):
    parts = []
    for _ in range(count):
        part = x.astype(BF16)
        parts.append(part)
        x = x - part.astype(F32)
    return parts


def summed(triangle, x, count):
    return sum(dot(triangle, part, NN) for part in pieces(x, count))


def both(x):
    return jnp.concatenate([x, x], axis=1)


def swapped(x):
    return jnp.concatenate([x[:, WIDTH:], x[:, :WIDTH]], axis=1)


def remote(src, dst, send, recv, peer):
    return pltpu.make_async_remote_copy(
        src_ref=src, dst_ref=dst, send_sem=send, recv_sem=recv, device_id=peer, device_id_type=MESH_ID
    )


def kernel(
    nz, ny, nt,
    x_ref, w_ref, v_ref, gf_ref, gb_ref, slack_ref, extra_ref, scale_ref, cot_ref,
    dq_ref, dgf_ref, dgb_ref, dv_ref, dw_ref,
    xall, xturn, dec_y, dec_z, dec_line,
    out1, in1, mid1, got1, back1, state1,
    out2, in2, mid2, got2, back2, state2,
    wg, wg_in, wg_mid, wg_got,
    x_send, x_recv, dy_send, dy_recv, dz_send, dz_recv,
    a1s, a1r, b1s, b1r, c1s, c1r,
    a2s, a2r, b2s, b2r, c2s, c2r,
    ws, wr, zs, zr,
):
    z, y, t = lax.axis_index("sp_0"), lax.axis_index("sp_1"), lax.axis_index("tp")
    rows = WIDTH // ny
    length = v_ref.shape[0]
    width_in = x_ref.shape[1]

    def far_first(n):
        return sorted(range(1, n), key=lambda o: -min(o, n - o))

    def at_y(o):
        return lax.rem(y + o, ny)

    def at_z(o):
        return lax.rem(z + o, nz)

    partner = t + 1 - 2 * lax.rem(t, 2)
    chips = [lax.rem(t + 2 * o, nt) for o in far_first(nt // 2)]

    barrier = pltpu.get_barrier_semaphore()
    count = 0
    for o in range(1, nz):
        pl.semaphore_signal(barrier, inc=1, device_id={"sp_0": at_z(o)}, device_id_type=MESH_ID)
        count += 1
    for o in range(1, ny):
        pl.semaphore_signal(barrier, inc=1, device_id={"sp_1": at_y(o)}, device_id_type=MESH_ID)
        count += 1
    for k in [partner] + chips:
        pl.semaphore_signal(barrier, inc=1, device_id={"tp": k}, device_id_type=MESH_ID)
        count += 1

    sent = []

    def send(src, dst, send_sem, recv_sem, peer):
        copy = remote(src, dst, send_sem, recv_sem, peer)
        copy.start()
        sent.append(copy)

    def arrived(dst, send_sem, recv_sem, peer):
        remote(dst, dst, send_sem, recv_sem, peer).wait_recv()

    pre = jnp.concatenate([gf_ref[...], gb_ref[...]], axis=1).astype(F32)
    slack = jnp.concatenate([slack_ref[0:1, :], slack_ref[1:2, :]], axis=1)
    gate = jax.nn.sigmoid(-pre)
    key = slack * gate
    forget = jnp.log1p(-key)
    row_id = lax.broadcasted_iota(jnp.int32, (length, length), 0)
    col_id = lax.broadcasted_iota(jnp.int32, (length, length), 1)
    lower = row_id >= col_id
    upper = row_id <= col_id
    lower_ones = jnp.where(lower, 1.0, 0.0).astype(BF16)
    upper_ones = jnp.where(upper, 1.0, 0.0).astype(BF16)
    spikes_f = jnp.sum(jnp.where(lower, extra_ref[0], 0.0), axis=1, keepdims=True)
    spikes_b = jnp.sum(jnp.where(upper, extra_ref[1], 0.0), axis=1, keepdims=True)
    run = jnp.concatenate(
        [
            summed(lower_ones, forget[:, :WIDTH], 3) + spikes_f,
            summed(upper_ones, forget[:, WIDTH:], 3) + spikes_b,
        ],
        axis=1,
    )
    closing = jnp.concatenate([run[length - 1 :, :WIDTH], run[0:1, WIDTH:]], axis=1)
    to_end = jnp.exp(closing - run)
    key_end = (key * to_end).astype(BF16)
    v = v_ref[...]
    local = dot(v, key_end, TN)
    out1[...] = local.astype(BF16).reshape(ny, rows, 2 * WIDTH)
    dec_y[pl.ds(y, 1)] = closing[None]
    in1[pl.ds(y, 1)] = out1[pl.ds(y, 1)]

    pl.semaphore_wait(barrier, count)

    def first_phase(out, into, ss, rs):
        for o in far_first(ny):
            k = at_y(o)
            send(out.at[k], into.at[y], ss.at[o], rs.at[y], {"sp_1": k})

    def first_wait(into, ss, rs):
        for o in range(1, ny):
            k = at_y(o)
            arrived(into.at[k], ss.at[o], rs.at[k], {"sp_1": k})

    def line_fold(into, decays):
        up, down = [None] * ny, [None] * ny
        total = jnp.zeros((rows, WIDTH), F32)
        for k in range(ny):
            up[k] = total
            total = jnp.exp(decays[k][:, :WIDTH]) * total + into[k, :, :WIDTH].astype(F32)
        total_up = total
        total = jnp.zeros((rows, WIDTH), F32)
        for k in reversed(range(ny)):
            down[k] = total
            total = jnp.exp(decays[k][:, WIDTH:]) * total + into[k, :, WIDTH:].astype(F32)
        return up, down, total_up, total

    def second_phase(mid, got, totals, ss, rs):
        mid[0] = totals[0].astype(BF16)
        mid[1] = totals[1].astype(BF16)
        got[pl.ds(z, 1)] = jnp.zeros((1, rows, WIDTH), BF16)
        for o in far_first(nz):
            k = at_z(o)
            side = jnp.where(k > z, 0, 1)
            send(mid.at[side], got.at[z], ss.at[o], rs.at[z], {"sp_0": k})

    def second_wait(got, ss, rs):
        for o in range(1, nz):
            k = at_z(o)
            arrived(got.at[k], ss.at[o], rs.at[k], {"sp_0": k})

    def line_entry(got, decays):
        above = jnp.zeros((rows, WIDTH), F32)
        for k in range(nz):
            new = jnp.exp(decays[k][:, :WIDTH]) * above + got[k].astype(F32)
            above = jnp.where(k < z, new, above)
        below = jnp.zeros((rows, WIDTH), F32)
        for k in reversed(range(nz)):
            new = jnp.exp(decays[k][:, WIDTH:]) * below + got[k].astype(F32)
            below = jnp.where(k > z, new, below)
        return above, below

    def third_phase(back, state, entry, prefixes, decays, ss, rs):
        above, below = entry
        up, down = prefixes
        gone = jnp.zeros((1, WIDTH), F32)
        first = []
        for k in range(ny):
            first.append(jnp.exp(gone) * above + up[k])
            gone = gone + decays[k][:, :WIDTH]
        gone = jnp.zeros((1, WIDTH), F32)
        second = [None] * ny
        for k in reversed(range(ny)):
            second[k] = jnp.exp(gone) * below + down[k]
            gone = gone + decays[k][:, WIDTH:]
        for k in range(ny):
            back[k] = jnp.concatenate([first[k], second[k]], axis=1).astype(BF16)
        here = pl.ds(pl.multiple_of(y * rows, rows), rows)
        for o in far_first(ny):
            k = at_y(o)
            send(back.at[k], state.at[here, :], ss.at[o], rs.at[y], {"sp_1": k})
        state[here, :] = back[pl.ds(y, 1)].reshape(rows, 2 * WIDTH)

    def third_wait(state, ss, rs):
        for o in range(1, ny):
            k = at_y(o)
            there = pl.ds(pl.multiple_of(k * rows, rows), rows)
            arrived(state.at[there, :], ss.at[o], rs.at[k], {"sp_1": k})

    for o in far_first(ny):
        k = at_y(o)
        send(dec_y.at[y], dec_y.at[y], dy_send.at[o], dy_recv.at[y], {"sp_1": k})
    first_phase(out1, in1, a1s, a1r)
    for i, k in enumerate(chips):
        send(x_ref, xall.at[t], x_send.at[i], x_recv.at[t], {"tp": k})
    send(x_ref, xall.at[t], x_send.at[len(chips)], x_recv.at[t], {"tp": partner})
    xall[pl.ds(t, 1)] = x_ref[...][None]

    first_half = lax.broadcasted_iota(jnp.int32, (length, 2 * WIDTH), 0) < HALF
    centre = [run[HALF // 2 - 1 : HALF // 2], run[HALF + HALF // 2 - 1 : HALF + HALF // 2]]
    middle = jnp.where(first_half, centre[0], centre[1])
    grow = jnp.exp(run - middle)
    shrink = jnp.exp(middle - run)
    from_start = jnp.exp(run)
    keys = pair_of(key * shrink)
    step_f = jnp.exp(centre[1][:, :WIDTH] - centre[0][:, :WIDTH])
    step_b = jnp.exp(centre[0][:, WIDTH:] - centre[1][:, WIDTH:])

    for o in range(1, ny):
        k = at_y(o)
        arrived(dec_y.at[k], dy_send.at[o], dy_recv.at[k], {"sp_1": k})
    decays1 = [dec_y[k] for k in range(ny)]
    line_total = sum(decays1[1:], decays1[0])
    dec_z[pl.ds(z, 1)] = line_total[None]
    for o in far_first(nz):
        k = at_z(o)
        send(dec_z.at[z], dec_z.at[z], dz_send.at[o], dz_recv.at[z], {"sp_0": k})
    first_wait(in1, a1s, a1r)
    up, down, total_up, total_down = line_fold(in1, decays1)
    second_phase(mid1, got1, (total_up, total_down), b1s, b1r)

    for i, k in enumerate(chips):
        arrived(xall.at[k], x_send.at[i], x_recv.at[k], {"tp": k})
        send(xall.at[k], xall.at[k], x_send.at[len(chips) + 1 + i], x_recv.at[k], {"tp": partner})

    for o in range(1, nz):
        k = at_z(o)
        arrived(dec_z.at[k], dz_send.at[o], dz_recv.at[k], {"sp_0": k})
    second_wait(got1, b1s, b1r)
    lines1 = [dec_z[k] for k in range(nz)]
    entry = line_entry(got1, lines1)
    third_phase(back1, state1, entry, (up, down), decays1, c1s, c1r)

    for k in [partner] + [k + 1 - 2 * lax.rem(k, 2) for k in chips]:
        arrived(xall.at[k], x_send.at[0], x_recv.at[k], {"tp": partner})
    raw = jnp.zeros((length, WIDTH), F32)
    for k in range(nt):
        raw += dot(xall[k], w_ref[pl.ds(k * width_in, width_in), :], NN)
    raw = raw.astype(BF16).astype(F32)
    sig = jax.nn.sigmoid(raw)
    root = WIDTH**-0.5
    query = both(raw * sig * root)
    queries = query * grow
    query_in = pair_of(query * from_start)

    lo, hi = slice(0, HALF), slice(HALF, 2 * HALF)
    fw, bw = slice(0, WIDTH), slice(WIDTH, 2 * WIDTH)
    far_f = pair_of(queries[hi, fw] * step_f)
    far_b = pair_of(queries[lo, bw] * step_b)
    queries = pair_of(queries)
    low = lower[lo, lo]
    upp = upper[lo, lo]

    def near(a):
        return jnp.where(low, dot(cut(queries, a, fw), cut(keys, a, fw), NT), 0.0) + jnp.where(
            upp, dot(cut(queries, a, bw), cut(keys, a, bw), NT), 0.0
        )

    scores = jnp.concatenate(
        [
            jnp.concatenate([near(lo), dot(far_b, cut(keys, hi, bw), NT)], axis=1),
            jnp.concatenate([dot(far_f, cut(keys, lo, fw), NT), near(hi)], axis=1),
        ],
        axis=0,
    )
    scores = pair_of(scores)
    inside = dot(scores, v, NN)
    for k in range(nt):
        xturn[pl.ds(k * width_in, width_in), :] = xall[k].T

    third_wait(state1, c1s, c1r)
    state = state1[...]
    mixed = inside + dot(query_in, state, NT)
    inv = lax.rsqrt(jnp.mean(mixed * mixed, axis=1, keepdims=True) + EPS)
    weighted = cot_ref[...].astype(F32) * scale_ref[...]
    along = jnp.mean(weighted * mixed, axis=1, keepdims=True)
    grad_out = pair_of(inv * (weighted - mixed * (inv * inv * along)))

    sense = dot(grad_out, query_in, TN)
    out2[...] = swapped(sense).astype(BF16).reshape(ny, rows, 2 * WIDTH)
    in2[pl.ds(y, 1)] = out2[pl.ds(y, 1)]
    first_phase(out2, in2, a2s, a2r)

    cross = dot(grad_out, v, NT)
    cross_low = [pair_of(jnp.where(low, cross[a, a], 0.0)) for a in (lo, hi)]
    cross_upp = [pair_of(jnp.where(upp, cross[a, a], 0.0)) for a in (lo, hi)]
    cross_f, cross_b = pair_of(cross[hi, lo]), pair_of(cross[lo, hi])
    dq_f = jnp.concatenate(
        [
            dot(cross_low[0], cut(keys, lo, fw), NN),
            dot(cross_low[1], cut(keys, hi, fw), NN) + step_f * dot(cross_f, cut(keys, lo, fw), NN),
        ],
        axis=0,
    )
    dq_b = jnp.concatenate(
        [
            dot(cross_upp[0], cut(keys, lo, bw), NN) + step_b * dot(cross_b, cut(keys, hi, bw), NN),
            dot(cross_upp[1], cut(keys, hi, bw), NN),
        ],
        axis=0,
    )
    dq = grow * jnp.concatenate([dq_f, dq_b], axis=1) + from_start * dot(grad_out, state, NN)
    draw = (dq[:, fw] + dq[:, bw]) * (root * sig * (1.0 + raw * (1.0 - sig)))
    draw = draw.astype(BF16)
    dq_ref[...] = draw
    part = wg.shape[1] * wg.shape[2]
    for k in range(nz):
        wg[k] = dot(xturn[pl.ds(k * part, part), :], draw, NN).astype(BF16).reshape(wg.shape[1:])
    for o in far_first(ny):
        k = at_y(o)
        send(wg.at[:, k], wg_in.at[y], ws.at[o], wr.at[y], {"sp_1": k})

    decays2 = [swapped(d) for d in decays1]
    lines2 = [swapped(d) for d in lines1]
    first_wait(in2, a2s, a2r)
    up, down, total_up, total_down = line_fold(in2, decays2)
    second_phase(mid2, got2, (total_up, total_down), b2s, b2r)

    dv = dot(scores, grad_out, TN)
    dk_f = jnp.concatenate(
        [
            dot(cross_low[0], cut(queries, lo, fw), TN) + dot(cross_f, far_f, TN),
            dot(cross_low[1], cut(queries, hi, fw), TN),
        ],
        axis=0,
    )
    dk_b = jnp.concatenate(
        [
            dot(cross_upp[0], cut(queries, lo, bw), TN),
            dot(cross_upp[1], cut(queries, hi, bw), TN) + dot(cross_b, far_b, TN),
        ],
        axis=0,
    )
    dk = shrink * jnp.concatenate([dk_f, dk_b], axis=1)
    drift = query * dq - key * dk
    left = jnp.exp(closing) * state.astype(F32) + local

    second_wait(got2, b2s, b2r)
    entry = line_entry(got2, lines2)
    third_phase(back2, state2, entry, (up, down), decays2, c2s, c2r)

    for o in range(1, ny):
        k = at_y(o)
        arrived(wg_in.at[k], ws.at[o], wr.at[k], {"sp_1": k})
    acc = wg[:, pl.ds(y, 1)].astype(F32).reshape(wg_mid.shape)
    for o in range(1, ny):
        acc += wg_in[pl.ds(at_y(o), 1)].astype(F32).reshape(wg_mid.shape)
    wg_mid[...] = acc.astype(BF16)
    for o in far_first(nz):
        k = at_z(o)
        send(wg_mid.at[k], wg_got.at[z], zs.at[o], zr.at[z], {"sp_0": k})
    wg_got[pl.ds(z, 1)] = wg_mid[pl.ds(z, 1)]

    third_wait(state2, c2s, c2r)
    after = swapped(state2[...])
    dv_ref[...] = (dv + dot(key_end, after, NT)).astype(BF16)
    dk_end = to_end * dot(v, after, NN)
    ends = jnp.sum(after.astype(F32) * left, axis=0, keepdims=True)
    drift = drift - key * dk_end
    drift = jnp.concatenate(
        [summed(upper_ones, drift[:, fw], 2), summed(lower_ones, drift[:, bw], 2)], axis=1
    )
    dkey = dk + dk_end - (drift + ends) / (1.0 - key)
    dgate = -key * (1.0 - gate) * dkey
    dgf_ref[...] = dgate[:, fw]
    dgb_ref[...] = dgate[:, bw]

    for o in range(1, nz):
        k = at_z(o)
        arrived(wg_got.at[k], zs.at[o], zr.at[k], {"sp_0": k})
    total = wg_got[0].astype(F32)
    for k in range(1, nz):
        total += wg_got[k].astype(F32)
    dw_ref[...] = total

    for copy in sent:
        copy.wait_send()


def on_device(nz, ny, x, w, v, gf, gb, slack, extra, scale, cot):
    nt = w.shape[0] // x.shape[1]
    length = v.shape[0]
    rows = WIDTH // ny
    depth = w.shape[0] // (nz * ny)
    lanes = 2 * WIDTH
    dma = pltpu.SemaphoreType.DMA

    def scan_buffers():
        return [
            pltpu.VMEM((ny, rows, lanes), BF16),
            pltpu.VMEM((ny, rows, lanes), BF16),
            pltpu.VMEM((2, rows, WIDTH), BF16),
            pltpu.VMEM((nz, rows, WIDTH), BF16),
            pltpu.VMEM((ny, rows, lanes), BF16),
            pltpu.VMEM((WIDTH, lanes), BF16),
        ]

    vmem = pl.BlockSpec(memory_space=pltpu.VMEM)
    return pl.pallas_call(
        functools.partial(kernel, nz, ny, nt),
        out_shape=(
            jax.ShapeDtypeStruct((length, WIDTH), BF16),
            jax.ShapeDtypeStruct((length, WIDTH), F32),
            jax.ShapeDtypeStruct((length, WIDTH), F32),
            jax.ShapeDtypeStruct((length, WIDTH), BF16),
            jax.ShapeDtypeStruct((depth, WIDTH), F32),
        ),
        in_specs=[vmem] * 9,
        out_specs=[vmem] * 5,
        scratch_shapes=[
            pltpu.VMEM((nt, length, x.shape[1]), BF16),
            pltpu.VMEM((w.shape[0], length), BF16),
            pltpu.VMEM((ny, 1, lanes), F32),
            pltpu.VMEM((nz, 1, lanes), F32),
            pltpu.VMEM((8, lanes), F32),
        ]
        + scan_buffers()
        + scan_buffers()
        + [
            pltpu.VMEM((nz, ny, depth, WIDTH), BF16),
            pltpu.VMEM((ny, nz, depth, WIDTH), BF16),
            pltpu.VMEM((nz, depth, WIDTH), BF16),
            pltpu.VMEM((nz, depth, WIDTH), BF16),
            dma((nt,)), dma((nt,)), dma((ny,)), dma((ny,)), dma((nz,)), dma((nz,)),
        ]
        + [dma((n,)) for n in (ny, ny, nz, nz, ny, ny)] * 2
        + [dma((n,)) for n in (ny, ny, nz, nz)],
        compiler_params=pltpu.CompilerParams(collective_id=0, has_side_effects=True),
    )(x, w, v, gf, gb, slack, extra.transpose(0, 2, 1), scale.reshape(1, WIDTH), cot)


def solution(mesh):
    torus = Mesh(mesh.devices.reshape(NZ, NY, mesh.shape["tp"]), ("sp_0", "sp_1", "tp"))
    sp = ("sp_0", "sp_1")
    return jax.shard_map(
        functools.partial(on_device, NZ, NY),
        mesh=torus,
        in_specs=(
            P(sp, "tp"),
            P(None, "tp"),
            P(sp, "tp"),
            P(sp, "tp"),
            P(sp, "tp"),
            P(None, "tp"),
            P(None, sp, "tp"),
            P("tp"),
            P(sp, "tp"),
        ),
        out_specs=(P(sp, "tp"),) * 5,
        check_vma=False,
    )
```

time: 530 us -> 70.6 us (0.13)
  the two profiles are of different devices: /device:TPU:6 before, /device:TPU:8 now
where the time goes in v1:
time: 70.6 us; the launch traced here: 70.3 us
  Pallas kernels  65 us (92%)
  local copies, waits for them, and re-layouts  4.65 us (7%)
    pallas_call x1, Pallas kernels, on_device(): pl.pallas_call(functools.partial(kernel, nz, ny, nt), out_shape=(jax.Shap...  65 us
    unnamed x13, local copies, waits for them, and re-layouts  4.65 us

profile of v1, /device:TPU:8, one launch (start us, length us, event | category | flops | bytes accessed | tf_op | source)
XLA Modules:
  0.0 70.3 jit_solution(16936270411476800749)
XLA Ops:
  0.6 65.0 %shard_map.128 = (bf16[256,128]{1,0:T(8,128)(2,1)}, f32[256,128]{1,0:T(8,128)}, f32[256,128]{1,0:T(8,128)}, bf16[256,128]{1,0:T(8,128)(2,1)}, f32[32,128]{1,0:T(8,128)}) custom-call(bf16[256,384]{1,0:T(8,128)(2,1)} %x_ref.1, bf16[3072,128]{1,0:T(8,128)(2,1)} %w_ref.1, bf16[256,128]{1,0:T(8,128)(2,1)} %v_ref.1, bf16[256,128]{1,0:T(8,128)(2,1)} %gf_ref.1, ...), custom_call_target="tpu_custom_call" | custom-call | tf_op jit(solution)/shard_map/pallas_call | solution.py:436
  65.6 0.0 copy-start.1
  65.7 1.5 %copy.19 = bf16[256,128]{1,0:T(8,128)(2,1)} copy(bf16[256,128]{1,0:T(8,128)(2,1)} %get-tuple-element.10) | data formatting | bytes 131072
  67.2 0.0 copy-done.1
  67.2 0.0 copy-start
  67.2 0.7 copy.20
  67.8 0.3 copy-done
  68.1 0.0 copy-start.2
  68.1 0.7 copy.21
  68.8 0.2 copy-done.2
  69.0 0.0 copy-start.3
  69.0 0.6 copy.22
  69.6 0.1 copy-done.3
  69.7 0.6 copy.23
Async XLA Ops:
  65.6 1.5 %copy-start.1 = (f32[256,128]{1,0:T(8,128)S(1)}, f32[256,128]{1,0:T(8,128)}, u32[]{:S(2)}) copy-start(f32[256,128]{1,0:T(8,128)} %get-tuple-element.11) | copy-start | bytes 393220
  67.2 1.0 %copy-start = (f32[256,128]{1,0:T(8,128)S(1)}, f32[256,128]{1,0:T(8,128)}, u32[]{:S(2)}) copy-start(f32[256,128]{1,0:T(8,128)} %get-tuple-element.12) | copy-start | bytes 393220
  68.1 0.9 %copy-start.2 = (bf16[256,128]{1,0:T(8,128)(2,1)S(1)}, bf16[256,128]{1,0:T(8,128)(2,1)}, u32[]{:S(2)}) copy-start(bf16[256,128]{1,0:T(8,128)(2,1)} %get-tuple-element.13) | copy-start | bytes 196612
  69.0 0.7 %copy-start.3 = (f32[32,128]{1,0:T(8,128)S(1)}, f32[32,128]{1,0:T(8,128)}, u32[]{:S(2)}) copy-start(f32[32,128]{1,0:T(8,128)} %get-tuple-element.14) | copy-start | bytes 49156

commit v2 on v1

--- a/solution.py
+++ b/solution.py
@@ -11,6 +11,7 @@
 WIDTH = 128
 HALF = 128
 NZ, NY = 12, 8
+NEAR = 3
 EPS = 1e-6
 MESH_ID = pl.DeviceIdType.MESH
 F32, BF16 = jnp.float32, jnp.bfloat16
@@ -68,21 +69,22 @@
 
 def kernel(
     nz, ny, nt,
-    x_ref, w_ref, v_ref, gf_ref, gb_ref, slack_ref, extra_ref, scale_ref, cot_ref,
+    x_hbm, w_hbm, v_hbm, gf_hbm, gb_hbm, slack_hbm, extra_hbm, scale_hbm, cot_hbm,
     dq_ref, dgf_ref, dgb_ref, dv_ref, dw_ref,
-    xall, xturn, dec_y, dec_z, dec_line,
+    w_ref, v_ref, gf_ref, gb_ref, slack_ref, extra_ref, scale_ref, cot_ref, load_sem,
+    xall, xturn, dec_y, dec_z,
     out1, in1, mid1, got1, back1, state1,
     out2, in2, mid2, got2, back2, state2,
-    wg, wg_in, wg_mid, wg_got,
+    wa, wa_in, wa_mid, wa_got, wb, wb_in, wb_mid, wb_got,
     x_send, x_recv, dy_send, dy_recv, dz_send, dz_recv,
     a1s, a1r, b1s, b1r, c1s, c1r,
     a2s, a2r, b2s, b2r, c2s, c2r,
-    ws, wr, zs, zr,
+    a3s, a3r, b3s, b3r, a4s, a4r, b4s, b4r,
 ):
     z, y, t = lax.axis_index("sp_0"), lax.axis_index("sp_1"), lax.axis_index("tp")
     rows = WIDTH // ny
     length = v_ref.shape[0]
-    width_in = x_ref.shape[1]
+    width_in = xall.shape[2]
 
     def far_first(n):
         return sorted(range(1, n), key=lambda o: -min(o, n - o))
@@ -108,6 +110,24 @@
         pl.semaphore_signal(barrier, inc=1, device_id={"tp": k}, device_id_type=MESH_ID)
         count += 1
 
+    loads = []
+    for i, (src, dst) in enumerate(
+        (
+            (gf_hbm, gf_ref),
+            (gb_hbm, gb_ref),
+            (slack_hbm, slack_ref),
+            (extra_hbm, extra_ref),
+            (v_hbm, v_ref),
+            (x_hbm, xall.at[t]),
+            (w_hbm, w_ref),
+            (cot_hbm, cot_ref),
+            (scale_hbm, scale_ref),
+        )
+    ):
+        load = pltpu.make_async_copy(src, dst, load_sem.at[i])
+        load.start()
+        loads.append(load)
+
     sent = []
 
     def send(src, dst, send_sem, recv_sem, peer):
@@ -118,6 +138,8 @@
     def arrived(dst, send_sem, recv_sem, peer):
         remote(dst, dst, send_sem, recv_sem, peer).wait_recv()
 
+    for load in loads[:4]:
+        load.wait()
     pre = jnp.concatenate([gf_ref[...], gb_ref[...]], axis=1).astype(F32)
     slack = jnp.concatenate([slack_ref[0:1, :], slack_ref[1:2, :]], axis=1)
     gate = jax.nn.sigmoid(-pre)
@@ -141,6 +163,7 @@
     closing = jnp.concatenate([run[length - 1 :, :WIDTH], run[0:1, WIDTH:]], axis=1)
     to_end = jnp.exp(closing - run)
     key_end = (key * to_end).astype(BF16)
+    loads[4].wait()
     v = v_ref[...]
     local = dot(v, key_end, TN)
     out1[...] = local.astype(BF16).reshape(ny, rows, 2 * WIDTH)
@@ -228,10 +251,10 @@
         k = at_y(o)
         send(dec_y.at[y], dec_y.at[y], dy_send.at[o], dy_recv.at[y], {"sp_1": k})
     first_phase(out1, in1, a1s, a1r)
+    loads[5].wait()
     for i, k in enumerate(chips):
-        send(x_ref, xall.at[t], x_send.at[i], x_recv.at[t], {"tp": k})
-    send(x_ref, xall.at[t], x_send.at[len(chips)], x_recv.at[t], {"tp": partner})
-    xall[pl.ds(t, 1)] = x_ref[...][None]
+        send(xall.at[t], xall.at[t], x_send.at[i], x_recv.at[t], {"tp": k})
+    send(xall.at[t], xall.at[t], x_send.at[len(chips)], x_recv.at[t], {"tp": partner})
 
     first_half = lax.broadcasted_iota(jnp.int32, (length, 2 * WIDTH), 0) < HALF
     centre = [run[HALF // 2 - 1 : HALF // 2], run[HALF + HALF // 2 - 1 : HALF + HALF // 2]]
@@ -256,10 +279,6 @@
     up, down, total_up, total_down = line_fold(in1, decays1)
     second_phase(mid1, got1, (total_up, total_down), b1s, b1r)
 
-    for i, k in enumerate(chips):
-        arrived(xall.at[k], x_send.at[i], x_recv.at[k], {"tp": k})
-        send(xall.at[k], xall.at[k], x_send.at[len(chips) + 1 + i], x_recv.at[k], {"tp": partner})
-
     for o in range(1, nz):
         k = at_z(o)
         arrived(dec_z.at[k], dz_send.at[o], dz_recv.at[k], {"sp_0": k})
@@ -268,8 +287,14 @@
     entry = line_entry(got1, lines1)
     third_phase(back1, state1, entry, (up, down), decays1, c1s, c1r)
 
+    for i, k in enumerate(chips):
+        arrived(xall.at[k], x_send.at[i], x_recv.at[k], {"tp": k})
+        send(xall.at[k], xall.at[k], x_send.at[len(chips) + 1 + i], x_recv.at[k], {"tp": partner})
+
     for k in [partner] + [k + 1 - 2 * lax.rem(k, 2) for k in chips]:
         arrived(xall.at[k], x_send.at[0], x_recv.at[k], {"tp": partner})
+    for load in loads[6:]:
+        load.wait()
     raw = jnp.zeros((length, WIDTH), F32)
     for k in range(nt):
         raw += dot(xall[k], w_ref[pl.ds(k * width_in, width_in), :], NN)
@@ -340,18 +365,30 @@
     draw = (dq[:, fw] + dq[:, bw]) * (root * sig * (1.0 + raw * (1.0 - sig)))
     draw = draw.astype(BF16)
     dq_ref[...] = draw
-    part = wg.shape[1] * wg.shape[2]
-    for k in range(nz):
-        wg[k] = dot(xturn[pl.ds(k * part, part), :], draw, NN).astype(BF16).reshape(wg.shape[1:])
+
+    part = ny * wa.shape[2]
+
+    def terms(o):
+        owner = pl.multiple_of(at_z(o) * part, part)
+        return dot(xturn[pl.ds(owner, part), :], draw, NN).astype(BF16).reshape(wa.shape[1:])
+
+    near_z = [o for o in range(1, nz) if min(o, nz - o) <= NEAR]
+    far_z = [o for o in range(nz) if o not in near_z]
+    for i, o in enumerate(far_z):
+        wa[i] = terms(o)
     for o in far_first(ny):
         k = at_y(o)
-        send(wg.at[:, k], wg_in.at[y], ws.at[o], wr.at[y], {"sp_1": k})
+        send(wa.at[:, k], wa_in.at[y], a3s.at[o], a3r.at[y], {"sp_1": k})
+    for i, o in enumerate(near_z):
+        wb[i] = terms(o)
 
     decays2 = [swapped(d) for d in decays1]
     lines2 = [swapped(d) for d in lines1]
     first_wait(in2, a2s, a2r)
     up, down, total_up, total_down = line_fold(in2, decays2)
     second_phase(mid2, got2, (total_up, total_down), b2s, b2r)
+    for i in sorted(range(len(near_z)), key=lambda i: -min(near_z[i], nz - near_z[i])):
+        send(wb.at[i], wb_in.at[i], b3s.at[i], b3r.at[i], {"sp_0": at_z(near_z[i])})
 
     dv = dot(scores, grad_out, TN)
     dk_f = jnp.concatenate(
@@ -378,15 +415,25 @@
 
     for o in range(1, ny):
         k = at_y(o)
-        arrived(wg_in.at[k], ws.at[o], wr.at[k], {"sp_1": k})
-    acc = wg[:, pl.ds(y, 1)].astype(F32).reshape(wg_mid.shape)
+        arrived(wa_in.at[k], a3s.at[o], a3r.at[k], {"sp_1": k})
+    acc = wa[:, pl.ds(y, 1)].astype(F32).reshape(wa_mid.shape)
     for o in range(1, ny):
-        acc += wg_in[pl.ds(at_y(o), 1)].astype(F32).reshape(wg_mid.shape)
-    wg_mid[...] = acc.astype(BF16)
-    for o in far_first(nz):
-        k = at_z(o)
-        send(wg_mid.at[k], wg_got.at[z], zs.at[o], zr.at[z], {"sp_0": k})
-    wg_got[pl.ds(z, 1)] = wg_mid[pl.ds(z, 1)]
+        acc += wa_in[pl.ds(at_y(o), 1)].astype(F32).reshape(wa_mid.shape)
+    own = acc[0]
+    wa_mid[...] = acc.astype(BF16)
+    for i in sorted(range(1, len(far_z)), key=lambda i: -min(far_z[i], nz - far_z[i])):
+        send(wa_mid.at[i], wa_got.at[i], b4s.at[i], b4r.at[i], {"sp_0": at_z(far_z[i])})
+
+    for i, o in enumerate(near_z):
+        arrived(wb_in.at[i], b3s.at[i], b3r.at[i], {"sp_0": at_z(nz - o)})
+    acc = wb_in[0].astype(F32)
+    for i in range(1, len(near_z)):
+        acc += wb_in[i].astype(F32)
+    wb_mid[...] = acc.astype(BF16)
+    for o in far_first(ny):
+        k = at_y(o)
+        send(wb_mid.at[k], wb_got.at[y], a4s.at[o], a4r.at[y], {"sp_1": k})
+    own += wb_mid[pl.ds(y, 1)].astype(F32).reshape(own.shape)
 
     third_wait(state2, c2s, c2r)
     after = swapped(state2[...])
@@ -402,16 +449,33 @@
     dgf_ref[...] = dgate[:, fw]
     dgb_ref[...] = dgate[:, bw]
 
-    for o in range(1, nz):
-        k = at_z(o)
-        arrived(wg_got.at[k], zs.at[o], zr.at[k], {"sp_0": k})
-    total = wg_got[0].astype(F32)
-    for k in range(1, nz):
-        total += wg_got[k].astype(F32)
-    dw_ref[...] = total
+    for i in range(1, len(far_z)):
+        arrived(wa_got.at[i], b4s.at[i], b4r.at[i], {"sp_0": at_z(nz - far_z[i])})
+        own += wa_got[i].astype(F32)
+    for o in range(1, ny):
+        k = at_y(o)
+        arrived(wb_got.at[k], a4s.at[o], a4r.at[k], {"sp_1": k})
+        own += wb_got[pl.ds(k, 1)].astype(F32).reshape(own.shape)
+    dw_ref[...] = own
 
     for copy in sent:
         copy.wait_send()
+
+
+def store(*refs):
+    sources, targets, sems = refs[:5], refs[5:10], refs[10]
+    copies = [
+        pltpu.make_async_copy(src, dst, sems.at[i])
+        for i, (src, dst) in enumerate(zip(sources, targets))
+    ]
+    for copy in copies:
+        copy.start()
+    for copy in copies:
+        copy.wait()
+
+
+def in_vmem(a):
+    return pltpu.with_memory_space_constraint(a, pltpu.VMEM)
 
 
 def on_device(nz, ny, x, w, v, gf, gb, slack, extra, scale, cot):
@@ -432,38 +496,61 @@
             pltpu.VMEM((WIDTH, lanes), BF16),
         ]
 
+    results = (
+        ((length, WIDTH), BF16),
+        ((length, WIDTH), F32),
+        ((length, WIDTH), F32),
+        ((length, WIDTH), BF16),
+        ((depth, WIDTH), F32),
+    )
+    near = sum(1 for o in range(1, nz) if min(o, nz - o) <= NEAR)
+    far = nz - near
     vmem = pl.BlockSpec(memory_space=pltpu.VMEM)
-    return pl.pallas_call(
+    anywhere = pl.BlockSpec(memory_space=pl.ANY)
+    held = pl.pallas_call(
         functools.partial(kernel, nz, ny, nt),
-        out_shape=(
-            jax.ShapeDtypeStruct((length, WIDTH), BF16),
-            jax.ShapeDtypeStruct((length, WIDTH), F32),
-            jax.ShapeDtypeStruct((length, WIDTH), F32),
-            jax.ShapeDtypeStruct((length, WIDTH), BF16),
-            jax.ShapeDtypeStruct((depth, WIDTH), F32),
-        ),
-        in_specs=[vmem] * 9,
+        out_shape=tuple(pltpu.VMEM(shape, dtype) for shape, dtype in results),
+        in_specs=[anywhere] * 9,
         out_specs=[vmem] * 5,
         scratch_shapes=[
+            pltpu.VMEM(w.shape, BF16),
+            pltpu.VMEM(v.shape, BF16),
+            pltpu.VMEM(gf.shape, BF16),
+            pltpu.VMEM(gb.shape, BF16),
+            pltpu.VMEM(slack.shape, F32),
+            pltpu.VMEM((2, 1, length), F32),
+            pltpu.VMEM((1, WIDTH), F32),
+            pltpu.VMEM(cot.shape, BF16),
+            dma((9,)),
             pltpu.VMEM((nt, length, x.shape[1]), BF16),
             pltpu.VMEM((w.shape[0], length), BF16),
             pltpu.VMEM((ny, 1, lanes), F32),
             pltpu.VMEM((nz, 1, lanes), F32),
-            pltpu.VMEM((8, lanes), F32),
         ]
         + scan_buffers()
         + scan_buffers()
         + [
-            pltpu.VMEM((nz, ny, depth, WIDTH), BF16),
-            pltpu.VMEM((ny, nz, depth, WIDTH), BF16),
-            pltpu.VMEM((nz, depth, WIDTH), BF16),
-            pltpu.VMEM((nz, depth, WIDTH), BF16),
+            pltpu.VMEM((far, ny, depth, WIDTH), BF16),
+            pltpu.VMEM((ny, far, depth, WIDTH), BF16),
+            pltpu.VMEM((far, depth, WIDTH), BF16),
+            pltpu.VMEM((far, depth, WIDTH), BF16),
+            pltpu.VMEM((near, ny, depth, WIDTH), BF16),
+            pltpu.VMEM((near, ny, depth, WIDTH), BF16),
+            pltpu.VMEM((ny, depth, WIDTH), BF16),
+            pltpu.VMEM((ny, depth, WIDTH), BF16),
             dma((nt,)), dma((nt,)), dma((ny,)), dma((ny,)), dma((nz,)), dma((nz,)),
         ]
         + [dma((n,)) for n in (ny, ny, nz, nz, ny, ny)] * 2
-        + [dma((n,)) for n in (ny, ny, nz, nz)],
+        + [dma((n,)) for n in (ny, ny, near, near, ny, ny, far, far)],
         compiler_params=pltpu.CompilerParams(collective_id=0, has_side_effects=True),
     )(x, w, v, gf, gb, slack, extra.transpose(0, 2, 1), scale.reshape(1, WIDTH), cot)
+    return pl.pallas_call(
+        store,
+        out_shape=tuple(jax.ShapeDtypeStruct(shape, dtype) for shape, dtype in results),
+        in_specs=[vmem] * 5,
+        out_specs=[anywhere] * 5,
+        scratch_shapes=[dma((5,))],
+    )(*(in_vmem(a) for a in held))
 
 
 def solution(mesh):

time: 70.6 us -> 59.8 us (0.85)
  the two profiles are of different devices: /device:TPU:8 before, /device:TPU:6 now
where the time goes in v2:
time: 59.8 us; the launch traced here: 59.6 us
  Pallas kernels  59 us (99%)
  between operations  0.64 us (1%)
    pallas_call x1, Pallas kernels, on_device(): pl.pallas_call(functools.partial(kernel, nz, ny, nt), out_shape=tuple((pl...  58.2 us

profile of v2, /device:TPU:6, one launch (start us, length us, event | category | flops | bytes accessed | tf_op | source)
XLA Modules:
  0.0 59.6 jit_solution(6338014534508493587)
XLA Ops:
  0.6 58.2 %shard_map.128 = (bf16[256,128]{1,0:T(8,128)(2,1)S(1)}, f32[256,128]{1,0:T(8,128)S(1)}, f32[256,128]{1,0:T(8,128)S(1)}, bf16[256,128]{1,0:T(8,128)(2,1)S(1)}, f32[32,128]{1,0:T(8,128)S(1)}) custom-call(bf16[256,384]{1,0:T(8,128)(2,1)} %x_hbm.1, bf16[3072,128]{1,0:T(8,128)(2,1)} %w_hbm.1, bf16[256,128]{1,0:T(8,128)(2,1)} %v_hbm.1, bf16[256,128]{1,0:T(8,128)(2,1)} %gf_hbm.1, ...), custom_call_target="tpu_custom_call" | custom-call | tf_op jit(solution)/shard_map/pallas_call | solution.py:510
  58.8 0.8 %shard_map.129 = (bf16[256,128]{1,0:T(8,128)(2,1)}, f32[256,128]{1,0:T(8,128)}, f32[256,128]{1,0:T(8,128)}, bf16[256,128]{1,0:T(8,128)(2,1)}, f32[32,128]{1,0:T(8,128)}) custom-call(bf16[256,128]{1,0:T(8,128)(2,1)S(1)} %get-tuple-element.10.refs_0_, f32[256,128]{1,0:T(8,128)S(1)} %get-tuple-element.11.refs_1_, f32[256,128]{1,0:T(8,128)S(1)} %get-tuple-element.12.refs_2_, ...), custom_call_target="tpu_custom_call" | custom-call | tf_op jit(solution)/shard_map/pallas_call | solution.py:547

commit v3 on v2

--- a/solution.py
+++ b/solution.py
@@ -11,7 +11,8 @@
 WIDTH = 128
 HALF = 128
 NZ, NY = 12, 8
-NEAR = 3
+NEAR = 2
+GROUPS = (2, 2)
 EPS = 1e-6
 MESH_ID = pl.DeviceIdType.MESH
 F32, BF16 = jnp.float32, jnp.bfloat16
@@ -367,28 +368,70 @@
     dq_ref[...] = draw
 
     part = ny * wa.shape[2]
-
-    def terms(o):
-        owner = pl.multiple_of(at_z(o) * part, part)
-        return dot(xturn[pl.ds(owner, part), :], draw, NN).astype(BF16).reshape(wa.shape[1:])
-
-    near_z = [o for o in range(1, nz) if min(o, nz - o) <= NEAR]
-    far_z = [o for o in range(nz) if o not in near_z]
-    for i, o in enumerate(far_z):
-        wa[i] = terms(o)
-    for o in far_first(ny):
-        k = at_y(o)
-        send(wa.at[:, k], wa_in.at[y], a3s.at[o], a3r.at[y], {"sp_1": k})
-    for i, o in enumerate(near_z):
-        wb[i] = terms(o)
+    far, near = nz - 2 * NEAR - 1, 2 * NEAR
+    far_turn = sum(jnp.where(z + NEAR + 1 + i < nz, 1, 0) for i in range(far))
+    near_at = [i + 1 + (nz - 1 - 2 * NEAR) * (i // NEAR) for i in range(near)]
+    near_turn = sum(jnp.where(z + o < nz, 1, 0) for o in near_at)
+    first, second = GROUPS
+    slots = [*range(first + second), None, *range(first + second, far)]
+    groups = [slice(0, first), slice(first, first + second + 1), slice(first + second + 1, far + 1)]
+
+    def far_index(rank):
+        return lax.rem(far_turn + rank, far)
+
+    def far_owner(index):
+        return lax.rem(z + NEAR + 1 + index, nz)
+
+    def terms(owner):
+        start = pl.multiple_of(owner * part, part)
+        return dot(xturn[pl.ds(start, part), :], draw, NN).astype(BF16).reshape(wa.shape[1:])
+
+    def far_send(g):
+        for o in far_first(ny):
+            k = at_y(o)
+            send(wa.at[groups[g], k], wa_in.at[y, groups[g]], a3s.at[g, o], a3r.at[g, y], {"sp_1": k})
+
+    def far_pass(g):
+        for o in range(1, ny):
+            k = at_y(o)
+            arrived(wa_in.at[k, groups[g]], a3s.at[g, o], a3r.at[g, k], {"sp_1": k})
+        count = groups[g].stop - groups[g].start
+        acc = wa[groups[g], pl.ds(y, 1)].astype(F32).reshape(count, *wa_mid.shape[1:])
+        for o in range(1, ny):
+            acc += wa_in[pl.ds(at_y(o), 1), groups[g]].astype(F32).reshape(acc.shape)
+        wa_mid[groups[g]] = acc.astype(BF16)
+        kept = None
+        for n, rank in enumerate(slots[groups[g]]):
+            slot = groups[g].start + n
+            if rank is None:
+                kept = acc[n]
+            else:
+                i = far_index(rank)
+                send(wa_mid.at[slot], wa_got.at[i], b4s.at[rank], b4r.at[i], {"sp_0": far_owner(i)})
+        return kept
+
+    def fill(g):
+        for slot in range(groups[g].start, groups[g].stop):
+            wa[slot] = terms(z if slots[slot] is None else far_owner(far_index(slots[slot])))
+
+    fill(0)
+    far_send(0)
+    fill(1)
+    far_send(1)
+    fill(2)
+    far_send(2)
+    for i, o in enumerate(near_at):
+        wb[i] = terms(at_z(o))
 
     decays2 = [swapped(d) for d in decays1]
     lines2 = [swapped(d) for d in lines1]
     first_wait(in2, a2s, a2r)
     up, down, total_up, total_down = line_fold(in2, decays2)
     second_phase(mid2, got2, (total_up, total_down), b2s, b2r)
-    for i in sorted(range(len(near_z)), key=lambda i: -min(near_z[i], nz - near_z[i])):
-        send(wb.at[i], wb_in.at[i], b3s.at[i], b3r.at[i], {"sp_0": at_z(near_z[i])})
+    for rank in range(near):
+        i = lax.rem(near_turn + rank, near)
+        o = i + 1 + (nz - 1 - 2 * NEAR) * (i // NEAR)
+        send(wb.at[i], wb_in.at[i], b3s.at[rank], b3r.at[i], {"sp_0": lax.rem(z + o, nz)})
 
     dv = dot(scores, grad_out, TN)
     dk_f = jnp.concatenate(
@@ -409,31 +452,22 @@
     drift = query * dq - key * dk
     left = jnp.exp(closing) * state.astype(F32) + local
 
+    far_pass(0)
     second_wait(got2, b2s, b2r)
     entry = line_entry(got2, lines2)
     third_phase(back2, state2, entry, (up, down), decays2, c2s, c2r)
 
-    for o in range(1, ny):
-        k = at_y(o)
-        arrived(wa_in.at[k], a3s.at[o], a3r.at[k], {"sp_1": k})
-    acc = wa[:, pl.ds(y, 1)].astype(F32).reshape(wa_mid.shape)
-    for o in range(1, ny):
-        acc += wa_in[pl.ds(at_y(o), 1)].astype(F32).reshape(wa_mid.shape)
-    own = acc[0]
-    wa_mid[...] = acc.astype(BF16)
-    for i in sorted(range(1, len(far_z)), key=lambda i: -min(far_z[i], nz - far_z[i])):
-        send(wa_mid.at[i], wa_got.at[i], b4s.at[i], b4r.at[i], {"sp_0": at_z(far_z[i])})
-
-    for i, o in enumerate(near_z):
+    for i, o in enumerate(near_at):
         arrived(wb_in.at[i], b3s.at[i], b3r.at[i], {"sp_0": at_z(nz - o)})
     acc = wb_in[0].astype(F32)
-    for i in range(1, len(near_z)):
+    for i in range(1, near):
         acc += wb_in[i].astype(F32)
     wb_mid[...] = acc.astype(BF16)
     for o in far_first(ny):
         k = at_y(o)
         send(wb_mid.at[k], wb_got.at[y], a4s.at[o], a4r.at[y], {"sp_1": k})
-    own += wb_mid[pl.ds(y, 1)].astype(F32).reshape(own.shape)
+    own = far_pass(1) + wb_mid[pl.ds(y, 1)].astype(F32).reshape(dw_ref.shape)
+    far_pass(2)
 
     third_wait(state2, c2s, c2r)
     after = swapped(state2[...])
@@ -449,8 +483,8 @@
     dgf_ref[...] = dgate[:, fw]
     dgb_ref[...] = dgate[:, bw]
 
-    for i in range(1, len(far_z)):
-        arrived(wa_got.at[i], b4s.at[i], b4r.at[i], {"sp_0": at_z(nz - far_z[i])})
+    for i in range(far):
+        arrived(wa_got.at[i], b4s.at[i], b4r.at[i], {"sp_0": at_z(nz - NEAR - 1 - i)})
         own += wa_got[i].astype(F32)
     for o in range(1, ny):
         k = at_y(o)
@@ -503,8 +537,7 @@
         ((length, WIDTH), BF16),
         ((depth, WIDTH), F32),
     )
-    near = sum(1 for o in range(1, nz) if min(o, nz - o) <= NEAR)
-    far = nz - near
+    near, far = 2 * NEAR, nz - 2 * NEAR - 1
     vmem = pl.BlockSpec(memory_space=pltpu.VMEM)
     anywhere = pl.BlockSpec(memory_space=pl.ANY)
     held = pl.pallas_call(
@@ -530,9 +563,9 @@
         + scan_buffers()
         + scan_buffers()
         + [
-            pltpu.VMEM((far, ny, depth, WIDTH), BF16),
-            pltpu.VMEM((ny, far, depth, WIDTH), BF16),
-            pltpu.VMEM((far, depth, WIDTH), BF16),
+            pltpu.VMEM((far + 1, ny, depth, WIDTH), BF16),
+            pltpu.VMEM((ny, far + 1, depth, WIDTH), BF16),
+            pltpu.VMEM((far + 1, depth, WIDTH), BF16),
             pltpu.VMEM((far, depth, WIDTH), BF16),
             pltpu.VMEM((near, ny, depth, WIDTH), BF16),
             pltpu.VMEM((near, ny, depth, WIDTH), BF16),
@@ -541,7 +574,7 @@
             dma((nt,)), dma((nt,)), dma((ny,)), dma((ny,)), dma((nz,)), dma((nz,)),
         ]
         + [dma((n,)) for n in (ny, ny, nz, nz, ny, ny)] * 2
-        + [dma((n,)) for n in (ny, ny, near, near, ny, ny, far, far)],
+        + [dma(n) for n in ((3, ny), (3, ny), (near,), (near,), (ny,), (ny,), (far,), (far,))],
         compiler_params=pltpu.CompilerParams(collective_id=0, has_side_effects=True),
     )(x, w, v, gf, gb, slack, extra.transpose(0, 2, 1), scale.reshape(1, WIDTH), cot)
     return pl.pallas_call(

time: 59.8 us -> 55.9 us (0.935); the launches traced: 59.6 us -> 54.8 us
  Pallas kernels: 59 us -> 54.1 us
    pallas_call x1, Pallas kernels: 58.2 us -> 53.3 us  [on_device(): pl.pallas_call(functools.partial(kernel, nz, ny, nt), out_shape=tuple((pl...]
where the time goes in v3:
time: 55.9 us; the launch traced here: 54.8 us
  Pallas kernels  54.1 us (97%)
  between operations  0.64 us (1%)
    pallas_call x1, Pallas kernels, on_device(): pl.pallas_call(functools.partial(kernel, nz, ny, nt), out_shape=tuple((pl...  53.3 us

profile of v3, /device:TPU:6, one launch (start us, length us, event | category | flops | bytes accessed | tf_op | source)
XLA Modules:
  0.0 54.8 jit_solution(12676994722217463805)
XLA Ops:
  0.6 53.3 %shard_map.128 = (bf16[256,128]{1,0:T(8,128)(2,1)S(1)}, f32[256,128]{1,0:T(8,128)S(1)}, f32[256,128]{1,0:T(8,128)S(1)}, bf16[256,128]{1,0:T(8,128)(2,1)S(1)}, f32[32,128]{1,0:T(8,128)S(1)}) custom-call(bf16[256,384]{1,0:T(8,128)(2,1)} %x_hbm.1, bf16[3072,128]{1,0:T(8,128)(2,1)} %w_hbm.1, bf16[256,128]{1,0:T(8,128)(2,1)} %v_hbm.1, bf16[256,128]{1,0:T(8,128)(2,1)} %gf_hbm.1, ...), custom_call_target="tpu_custom_call" | custom-call | tf_op jit(solution)/shard_map/pallas_call | solution.py:543
  54.0 0.8 %shard_map.129 = (bf16[256,128]{1,0:T(8,128)(2,1)}, f32[256,128]{1,0:T(8,128)}, f32[256,128]{1,0:T(8,128)}, bf16[256,128]{1,0:T(8,128)(2,1)}, f32[32,128]{1,0:T(8,128)}) custom-call(bf16[256,128]{1,0:T(8,128)(2,1)S(1)} %get-tuple-element.10.refs_0_, f32[256,128]{1,0:T(8,128)S(1)} %get-tuple-element.11.refs_1_, f32[256,128]{1,0:T(8,128)S(1)} %get-tuple-element.12.refs_2_, ...), custom_call_target="tpu_custom_call" | custom-call | tf_op jit(solution)/shard_map/pallas_call | solution.py:580

commit v4 on v3

--- a/solution.py
+++ b/solution.py
@@ -11,8 +11,9 @@
 WIDTH = 128
 HALF = 128
 NZ, NY = 12, 8
-NEAR = 2
-GROUPS = (2, 2)
+NEAR = 3
+GROUPS = (2, 1)
+EARLY = 1
 EPS = 1e-6
 MESH_ID = pl.DeviceIdType.MESH
 F32, BF16 = jnp.float32, jnp.bfloat16
@@ -66,6 +67,9 @@
     return pltpu.make_async_remote_copy(
         src_ref=src, dst_ref=dst, send_sem=send, recv_sem=recv, device_id=peer, device_id_type=MESH_ID
     )
+
+
+EXCHANGES = ("dy", "a1", "dz", "b1", "c1", "a2", "b2", "c2", "g0", "g1", "g2", "b3", "a4", "b4", "xo", "xf")
 
 
 def kernel(
@@ -77,10 +81,7 @@
     out1, in1, mid1, got1, back1, state1,
     out2, in2, mid2, got2, back2, state2,
     wa, wa_in, wa_mid, wa_got, wb, wb_in, wb_mid, wb_got,
-    x_send, x_recv, dy_send, dy_recv, dz_send, dz_recv,
-    a1s, a1r, b1s, b1r, c1s, c1r,
-    a2s, a2r, b2s, b2r, c2s, c2r,
-    a3s, a3r, b3s, b3r, a4s, a4r, b4s, b4r,
+    send_sem, recv_sem,
 ):
     z, y, t = lax.axis_index("sp_0"), lax.axis_index("sp_1"), lax.axis_index("tp")
     rows = WIDTH // ny
@@ -97,7 +98,8 @@
         return lax.rem(z + o, nz)
 
     partner = t + 1 - 2 * lax.rem(t, 2)
-    chips = [lax.rem(t + 2 * o, nt) for o in far_first(nt // 2)]
+    steps = far_first(nt // 2)
+    chips = [lax.rem(t + 2 * o, nt) for o in steps]
 
     barrier = pltpu.get_barrier_semaphore()
     count = 0
@@ -129,15 +131,22 @@
         load.start()
         loads.append(load)
 
-    sent = []
-
-    def send(src, dst, send_sem, recv_sem, peer):
-        copy = remote(src, dst, send_sem, recv_sem, peer)
-        copy.start()
-        sent.append(copy)
-
-    def arrived(dst, send_sem, recv_sem, peer):
-        remote(dst, dst, send_sem, recv_sem, peer).wait_recv()
+    def send(name, src, dst, peer, chip=None):
+        n = EXCHANGES.index(name)
+        m = n if chip is None else len(EXCHANGES) + chip
+        remote(src, dst, send_sem.at[n], recv_sem.at[m], peer).start()
+
+    def arrived(name, whole, peer, chip=None):
+        n = EXCHANGES.index(name)
+        m = n if chip is None else len(EXCHANGES) + chip
+        remote(whole, whole, send_sem.at[n], recv_sem.at[m], peer).wait_recv()
+
+    def gone(name, whole, peer):
+        n = EXCHANGES.index(name)
+        remote(whole, whole, send_sem.at[n], recv_sem.at[n], peer).wait_send()
+
+    next_y, next_z = {"sp_1": at_y(1)}, {"sp_0": at_z(1)}
+    others_y, others_z = pl.ds(0, ny - 1), pl.ds(0, nz - 1)
 
     for load in loads[:4]:
         load.wait()
@@ -173,15 +182,10 @@
 
     pl.semaphore_wait(barrier, count)
 
-    def first_phase(out, into, ss, rs):
+    def first_phase(name, out, into):
         for o in far_first(ny):
             k = at_y(o)
-            send(out.at[k], into.at[y], ss.at[o], rs.at[y], {"sp_1": k})
-
-    def first_wait(into, ss, rs):
-        for o in range(1, ny):
-            k = at_y(o)
-            arrived(into.at[k], ss.at[o], rs.at[k], {"sp_1": k})
+            send(name, out.at[k], into.at[y], {"sp_1": k})
 
     def line_fold(into, decays):
         up, down = [None] * ny, [None] * ny
@@ -196,19 +200,14 @@
             total = jnp.exp(decays[k][:, WIDTH:]) * total + into[k, :, WIDTH:].astype(F32)
         return up, down, total_up, total
 
-    def second_phase(mid, got, totals, ss, rs):
+    def second_phase(name, mid, got, totals):
         mid[0] = totals[0].astype(BF16)
         mid[1] = totals[1].astype(BF16)
         got[pl.ds(z, 1)] = jnp.zeros((1, rows, WIDTH), BF16)
         for o in far_first(nz):
             k = at_z(o)
             side = jnp.where(k > z, 0, 1)
-            send(mid.at[side], got.at[z], ss.at[o], rs.at[z], {"sp_0": k})
-
-    def second_wait(got, ss, rs):
-        for o in range(1, nz):
-            k = at_z(o)
-            arrived(got.at[k], ss.at[o], rs.at[k], {"sp_0": k})
+            send(name, mid.at[side], got.at[z], {"sp_0": k})
 
     def line_entry(got, decays):
         above = jnp.zeros((rows, WIDTH), F32)
@@ -221,41 +220,34 @@
             below = jnp.where(k > z, new, below)
         return above, below
 
-    def third_phase(back, state, entry, prefixes, decays, ss, rs):
+    def third_phase(name, back, state, entry, prefixes, decays):
         above, below = entry
         up, down = prefixes
-        gone = jnp.zeros((1, WIDTH), F32)
+        past = jnp.zeros((1, WIDTH), F32)
         first = []
         for k in range(ny):
-            first.append(jnp.exp(gone) * above + up[k])
-            gone = gone + decays[k][:, :WIDTH]
-        gone = jnp.zeros((1, WIDTH), F32)
+            first.append(jnp.exp(past) * above + up[k])
+            past = past + decays[k][:, :WIDTH]
+        past = jnp.zeros((1, WIDTH), F32)
         second = [None] * ny
         for k in reversed(range(ny)):
-            second[k] = jnp.exp(gone) * below + down[k]
-            gone = gone + decays[k][:, WIDTH:]
+            second[k] = jnp.exp(past) * below + down[k]
+            past = past + decays[k][:, WIDTH:]
         for k in range(ny):
             back[k] = jnp.concatenate([first[k], second[k]], axis=1).astype(BF16)
         here = pl.ds(pl.multiple_of(y * rows, rows), rows)
         for o in far_first(ny):
             k = at_y(o)
-            send(back.at[k], state.at[here, :], ss.at[o], rs.at[y], {"sp_1": k})
+            send(name, back.at[k], state.at[here, :], {"sp_1": k})
         state[here, :] = back[pl.ds(y, 1)].reshape(rows, 2 * WIDTH)
 
-    def third_wait(state, ss, rs):
-        for o in range(1, ny):
-            k = at_y(o)
-            there = pl.ds(pl.multiple_of(k * rows, rows), rows)
-            arrived(state.at[there, :], ss.at[o], rs.at[k], {"sp_1": k})
-
     for o in far_first(ny):
-        k = at_y(o)
-        send(dec_y.at[y], dec_y.at[y], dy_send.at[o], dy_recv.at[y], {"sp_1": k})
-    first_phase(out1, in1, a1s, a1r)
+        send("dy", dec_y.at[y], dec_y.at[y], {"sp_1": at_y(o)})
+    first_phase("a1", out1, in1)
     loads[5].wait()
     for i, k in enumerate(chips):
-        send(xall.at[t], xall.at[t], x_send.at[i], x_recv.at[t], {"tp": k})
-    send(xall.at[t], xall.at[t], x_send.at[len(chips)], x_recv.at[t], {"tp": partner})
+        send("xo", xall.at[t], xall.at[t], {"tp": k}, i)
+    send("xo", xall.at[t], xall.at[t], {"tp": partner}, len(chips))
 
     first_half = lax.broadcasted_iota(jnp.int32, (length, 2 * WIDTH), 0) < HALF
     centre = [run[HALF // 2 - 1 : HALF // 2], run[HALF + HALF // 2 - 1 : HALF + HALF // 2]]
@@ -267,33 +259,28 @@
     step_f = jnp.exp(centre[1][:, :WIDTH] - centre[0][:, :WIDTH])
     step_b = jnp.exp(centre[0][:, WIDTH:] - centre[1][:, WIDTH:])
 
-    for o in range(1, ny):
-        k = at_y(o)
-        arrived(dec_y.at[k], dy_send.at[o], dy_recv.at[k], {"sp_1": k})
+    arrived("dy", dec_y.at[others_y], next_y)
     decays1 = [dec_y[k] for k in range(ny)]
     line_total = sum(decays1[1:], decays1[0])
     dec_z[pl.ds(z, 1)] = line_total[None]
     for o in far_first(nz):
-        k = at_z(o)
-        send(dec_z.at[z], dec_z.at[z], dz_send.at[o], dz_recv.at[z], {"sp_0": k})
-    first_wait(in1, a1s, a1r)
+        send("dz", dec_z.at[z], dec_z.at[z], {"sp_0": at_z(o)})
+    arrived("a1", in1.at[others_y], next_y)
     up, down, total_up, total_down = line_fold(in1, decays1)
-    second_phase(mid1, got1, (total_up, total_down), b1s, b1r)
-
-    for o in range(1, nz):
-        k = at_z(o)
-        arrived(dec_z.at[k], dz_send.at[o], dz_recv.at[k], {"sp_0": k})
-    second_wait(got1, b1s, b1r)
+    second_phase("b1", mid1, got1, (total_up, total_down))
+
+    arrived("dz", dec_z.at[others_z], next_z)
+    arrived("b1", got1.at[others_z], next_z)
     lines1 = [dec_z[k] for k in range(nz)]
     entry = line_entry(got1, lines1)
-    third_phase(back1, state1, entry, (up, down), decays1, c1s, c1r)
-
-    for i, k in enumerate(chips):
-        arrived(xall.at[k], x_send.at[i], x_recv.at[k], {"tp": k})
-        send(xall.at[k], xall.at[k], x_send.at[len(chips) + 1 + i], x_recv.at[k], {"tp": partner})
-
-    for k in [partner] + [k + 1 - 2 * lax.rem(k, 2) for k in chips]:
-        arrived(xall.at[k], x_send.at[0], x_recv.at[k], {"tp": partner})
+    third_phase("c1", back1, state1, entry, (up, down), decays1)
+
+    for o, k in zip(steps, chips):
+        arrived("xo", xall.at[k], {"tp": k}, steps.index(nt // 2 - o))
+        send("xf", xall.at[k], xall.at[k], {"tp": partner})
+    arrived("xo", xall.at[partner], {"tp": partner}, len(chips))
+    if chips:
+        arrived("xf", xall.at[pl.ds(0, len(chips))], {"tp": partner})
     for load in loads[6:]:
         load.wait()
     raw = jnp.zeros((length, WIDTH), F32)
@@ -331,7 +318,7 @@
     for k in range(nt):
         xturn[pl.ds(k * width_in, width_in), :] = xall[k].T
 
-    third_wait(state1, c1s, c1r)
+    arrived("c1", state1.at[pl.ds(0, WIDTH - rows), :], next_y)
     state = state1[...]
     mixed = inside + dot(query_in, state, NT)
     inv = lax.rsqrt(jnp.mean(mixed * mixed, axis=1, keepdims=True) + EPS)
@@ -342,7 +329,7 @@
     sense = dot(grad_out, query_in, TN)
     out2[...] = swapped(sense).astype(BF16).reshape(ny, rows, 2 * WIDTH)
     in2[pl.ds(y, 1)] = out2[pl.ds(y, 1)]
-    first_phase(out2, in2, a2s, a2r)
+    first_phase("a2", out2, in2)
 
     cross = dot(grad_out, v, NT)
     cross_low = [pair_of(jnp.where(low, cross[a, a], 0.0)) for a in (lo, hi)]
@@ -389,12 +376,10 @@
     def far_send(g):
         for o in far_first(ny):
             k = at_y(o)
-            send(wa.at[groups[g], k], wa_in.at[y, groups[g]], a3s.at[g, o], a3r.at[g, y], {"sp_1": k})
+            send(f"g{g}", wa.at[groups[g], k], wa_in.at[y, groups[g]], {"sp_1": k})
 
     def far_pass(g):
-        for o in range(1, ny):
-            k = at_y(o)
-            arrived(wa_in.at[k, groups[g]], a3s.at[g, o], a3r.at[g, k], {"sp_1": k})
+        arrived(f"g{g}", wa_in.at[others_y, groups[g]], next_y)
         count = groups[g].stop - groups[g].start
         acc = wa[groups[g], pl.ds(y, 1)].astype(F32).reshape(count, *wa_mid.shape[1:])
         for o in range(1, ny):
@@ -407,31 +392,41 @@
                 kept = acc[n]
             else:
                 i = far_index(rank)
-                send(wa_mid.at[slot], wa_got.at[i], b4s.at[rank], b4r.at[i], {"sp_0": far_owner(i)})
+                send("b4", wa_mid.at[slot], wa_got.at[i], {"sp_0": far_owner(i)})
         return kept
 
     def fill(g):
         for slot in range(groups[g].start, groups[g].stop):
             wa[slot] = terms(z if slots[slot] is None else far_owner(far_index(slots[slot])))
 
+    def near_send(ranks):
+        for rank in ranks:
+            i = lax.rem(near_turn + rank, near)
+            o = i + 1 + (nz - 1 - 2 * NEAR) * (i // NEAR)
+            send("b3", wb.at[i], wb_in.at[i], {"sp_0": lax.rem(z + o, nz)})
+
+    def near_fill(ranks):
+        for rank in ranks:
+            i = lax.rem(near_turn + rank, near)
+            o = i + 1 + (nz - 1 - 2 * NEAR) * (i // NEAR)
+            wb[pl.ds(i, 1)] = terms(lax.rem(z + o, nz))[None]
+
     fill(0)
     far_send(0)
+    near_fill(range(EARLY))
+    near_send(range(EARLY))
     fill(1)
     far_send(1)
     fill(2)
     far_send(2)
-    for i, o in enumerate(near_at):
-        wb[i] = terms(at_z(o))
+    near_fill(range(EARLY, near))
 
     decays2 = [swapped(d) for d in decays1]
     lines2 = [swapped(d) for d in lines1]
-    first_wait(in2, a2s, a2r)
+    arrived("a2", in2.at[others_y], next_y)
     up, down, total_up, total_down = line_fold(in2, decays2)
-    second_phase(mid2, got2, (total_up, total_down), b2s, b2r)
-    for rank in range(near):
-        i = lax.rem(near_turn + rank, near)
-        o = i + 1 + (nz - 1 - 2 * NEAR) * (i // NEAR)
-        send(wb.at[i], wb_in.at[i], b3s.at[rank], b3r.at[i], {"sp_0": lax.rem(z + o, nz)})
+    second_phase("b2", mid2, got2, (total_up, total_down))
+    near_send(range(EARLY, near))
 
     dv = dot(scores, grad_out, TN)
     dk_f = jnp.concatenate(
@@ -453,23 +448,23 @@
     left = jnp.exp(closing) * state.astype(F32) + local
 
     far_pass(0)
-    second_wait(got2, b2s, b2r)
+    arrived("b2", got2.at[others_z], next_z)
     entry = line_entry(got2, lines2)
-    third_phase(back2, state2, entry, (up, down), decays2, c2s, c2r)
-
-    for i, o in enumerate(near_at):
-        arrived(wb_in.at[i], b3s.at[i], b3r.at[i], {"sp_0": at_z(nz - o)})
+    third_phase("c2", back2, state2, entry, (up, down), decays2)
+
+    own = far_pass(1)
+    far_pass(2)
+    arrived("b3", wb_in, next_z)
     acc = wb_in[0].astype(F32)
     for i in range(1, near):
         acc += wb_in[i].astype(F32)
     wb_mid[...] = acc.astype(BF16)
     for o in far_first(ny):
         k = at_y(o)
-        send(wb_mid.at[k], wb_got.at[y], a4s.at[o], a4r.at[y], {"sp_1": k})
-    own = far_pass(1) + wb_mid[pl.ds(y, 1)].astype(F32).reshape(dw_ref.shape)
-    far_pass(2)
-
-    third_wait(state2, c2s, c2r)
+        send("a4", wb_mid.at[k], wb_got.at[y], {"sp_1": k})
+    own += wb_mid[pl.ds(y, 1)].astype(F32).reshape(dw_ref.shape)
+
+    arrived("c2", state2.at[pl.ds(0, WIDTH - rows), :], next_y)
     after = swapped(state2[...])
     dv_ref[...] = (dv + dot(key_end, after, NT)).astype(BF16)
     dk_end = to_end * dot(v, after, NN)
@@ -483,17 +478,37 @@
     dgf_ref[...] = dgate[:, fw]
     dgb_ref[...] = dgate[:, bw]
 
+    arrived("a4", wb_got.at[others_y], next_y)
+    for o in range(1, ny):
+        own += wb_got[pl.ds(at_y(o), 1)].astype(F32).reshape(own.shape)
+    arrived("b4", wa_got, next_z)
     for i in range(far):
-        arrived(wa_got.at[i], b4s.at[i], b4r.at[i], {"sp_0": at_z(nz - NEAR - 1 - i)})
         own += wa_got[i].astype(F32)
-    for o in range(1, ny):
-        k = at_y(o)
-        arrived(wb_got.at[k], a4s.at[o], a4r.at[k], {"sp_1": k})
-        own += wb_got[pl.ds(k, 1)].astype(F32).reshape(own.shape)
     dw_ref[...] = own
 
-    for copy in sent:
-        copy.wait_send()
+    for name, whole in (
+        ("dy", dec_y.at[others_y]),
+        ("a1", out1.at[others_y]),
+        ("c1", back1.at[others_y]),
+        ("a2", out2.at[others_y]),
+        ("c2", back2.at[others_y]),
+        ("g0", wa_in.at[others_y, groups[0]]),
+        ("g1", wa_in.at[others_y, groups[1]]),
+        ("g2", wa_in.at[others_y, groups[2]]),
+        ("a4", wb_got.at[others_y]),
+    ):
+        gone(name, whole, next_y)
+    for name, whole in (
+        ("dz", dec_z.at[others_z]),
+        ("b1", got1.at[others_z]),
+        ("b2", got2.at[others_z]),
+        ("b3", wb_in),
+        ("b4", wa_got),
+    ):
+        gone(name, whole, next_z)
+    gone("xo", xall.at[pl.ds(0, len(chips) + 1)], {"tp": partner})
+    if chips:
+        gone("xf", xall.at[pl.ds(0, len(chips))], {"tp": partner})
 
 
 def store(*refs):
@@ -571,10 +586,9 @@
             pltpu.VMEM((near, ny, depth, WIDTH), BF16),
             pltpu.VMEM((ny, depth, WIDTH), BF16),
             pltpu.VMEM((ny, depth, WIDTH), BF16),
-            dma((nt,)), dma((nt,)), dma((ny,)), dma((ny,)), dma((nz,)), dma((nz,)),
-        ]
-        + [dma((n,)) for n in (ny, ny, nz, nz, ny, ny)] * 2
-        + [dma(n) for n in ((3, ny), (3, ny), (near,), (near,), (ny,), (ny,), (far,), (far,))],
+            dma((len(EXCHANGES),)),
+            dma((len(EXCHANGES) + nt // 2,)),
+        ],
         compiler_params=pltpu.CompilerParams(collective_id=0, has_side_effects=True),
     )(x, w, v, gf, gb, slack, extra.transpose(0, 2, 1), scale.reshape(1, WIDTH), cot)
     return pl.pallas_call(

time: 55.9 us -> 55.2 us (0.987)
  the two profiles are of different devices: /device:TPU:6 before, /device:TPU:8 now
where the time goes in v4:
time: 55.2 us; the launch traced here: 55.1 us
  Pallas kernels  54.4 us (99%)
  between operations  0.64 us (1%)
    pallas_call x1, Pallas kernels, on_device(): pl.pallas_call(functools.partial(kernel, nz, ny, nt), out_shape=tuple((pl...  53.6 us

profile of v4, /device:TPU:8, one launch (start us, length us, event | category | flops | bytes accessed | tf_op | source)
XLA Modules:
  0.0 55.1 jit_solution(15754576692758063166)
XLA Ops:
  0.6 53.6 %shard_map.128 = (bf16[256,128]{1,0:T(8,128)(2,1)S(1)}, f32[256,128]{1,0:T(8,128)S(1)}, f32[256,128]{1,0:T(8,128)S(1)}, bf16[256,128]{1,0:T(8,128)(2,1)S(1)}, f32[32,128]{1,0:T(8,128)S(1)}) custom-call(bf16[256,384]{1,0:T(8,128)(2,1)} %x_hbm.1, bf16[3072,128]{1,0:T(8,128)(2,1)} %w_hbm.1, bf16[256,128]{1,0:T(8,128)(2,1)} %v_hbm.1, bf16[256,128]{1,0:T(8,128)(2,1)} %gf_hbm.1, ...), custom_call_target="tpu_custom_call" | custom-call | tf_op jit(solution)/shard_map/pallas_call | solution.py:558
  54.3 0.8 %shard_map.129 = (bf16[256,128]{1,0:T(8,128)(2,1)}, f32[256,128]{1,0:T(8,128)}, f32[256,128]{1,0:T(8,128)}, bf16[256,128]{1,0:T(8,128)(2,1)}, f32[32,128]{1,0:T(8,128)}) custom-call(bf16[256,128]{1,0:T(8,128)(2,1)S(1)} %get-tuple-element.10.refs_0_, f32[256,128]{1,0:T(8,128)S(1)} %get-tuple-element.11.refs_1_, f32[256,128]{1,0:T(8,128)S(1)} %get-tuple-element.12.refs_2_, ...), custom_call_target="tpu_custom_call" | custom-call | tf_op jit(solution)/shard_map/pallas_call | solution.py:594

commit v5 on v4

--- a/solution.py
+++ b/solution.py
@@ -13,7 +13,7 @@
 NZ, NY = 12, 8
 NEAR = 3
 GROUPS = (2, 1)
-EARLY = 1
+EARLY, MIDDLE = 1, 3
 EPS = 1e-6
 MESH_ID = pl.DeviceIdType.MESH
 F32, BF16 = jnp.float32, jnp.bfloat16
@@ -100,18 +100,6 @@
     partner = t + 1 - 2 * lax.rem(t, 2)
     steps = far_first(nt // 2)
     chips = [lax.rem(t + 2 * o, nt) for o in steps]
-
-    barrier = pltpu.get_barrier_semaphore()
-    count = 0
-    for o in range(1, nz):
-        pl.semaphore_signal(barrier, inc=1, device_id={"sp_0": at_z(o)}, device_id_type=MESH_ID)
-        count += 1
-    for o in range(1, ny):
-        pl.semaphore_signal(barrier, inc=1, device_id={"sp_1": at_y(o)}, device_id_type=MESH_ID)
-        count += 1
-    for k in [partner] + chips:
-        pl.semaphore_signal(barrier, inc=1, device_id={"tp": k}, device_id_type=MESH_ID)
-        count += 1
 
     loads = []
     for i, (src, dst) in enumerate(
@@ -130,6 +118,18 @@
         load = pltpu.make_async_copy(src, dst, load_sem.at[i])
         load.start()
         loads.append(load)
+
+    barrier = pltpu.get_barrier_semaphore()
+    count = 0
+    for o in far_first(nz):
+        pl.semaphore_signal(barrier, inc=1, device_id={"sp_0": at_z(o)}, device_id_type=MESH_ID)
+        count += 1
+    for o in range(1, ny):
+        pl.semaphore_signal(barrier, inc=1, device_id={"sp_1": at_y(o)}, device_id_type=MESH_ID)
+        count += 1
+    for k in [partner] + chips:
+        pl.semaphore_signal(barrier, inc=1, device_id={"tp": k}, device_id_type=MESH_ID)
+        count += 1
 
     def send(name, src, dst, peer, chip=None):
         n = EXCHANGES.index(name)
@@ -426,7 +426,7 @@
     arrived("a2", in2.at[others_y], next_y)
     up, down, total_up, total_down = line_fold(in2, decays2)
     second_phase("b2", mid2, got2, (total_up, total_down))
-    near_send(range(EARLY, near))
+    near_send(range(EARLY, MIDDLE))
 
     dv = dot(scores, grad_out, TN)
     dk_f = jnp.concatenate(
@@ -448,6 +448,7 @@
     left = jnp.exp(closing) * state.astype(F32) + local
 
     far_pass(0)
+    near_send(range(MIDDLE, near))
     arrived("b2", got2.at[others_z], next_z)
     entry = line_entry(got2, lines2)
     third_phase("c2", back2, state2, entry, (up, down), decays2)

time: 55.2 us -> 53.2 us (0.964)
  the two profiles are of different devices: /device:TPU:8 before, /device:TPU:128 now
where the time goes in v5:
time: 53.2 us; the launch traced here: 53.1 us
  Pallas kernels  52.5 us (99%)
  between operations  0.64 us (1%)
    pallas_call x1, Pallas kernels, on_device(): pl.pallas_call(functools.partial(kernel, nz, ny, nt), out_shape=tuple((pl...  51.7 us

profile of v5, /device:TPU:128, one launch (start us, length us, event | category | flops | bytes accessed | tf_op | source)
XLA Modules:
  0.0 53.1 jit_solution(13733470866459774788)
XLA Ops:
  0.6 51.7 %shard_map.128 = (bf16[256,128]{1,0:T(8,128)(2,1)S(1)}, f32[256,128]{1,0:T(8,128)S(1)}, f32[256,128]{1,0:T(8,128)S(1)}, bf16[256,128]{1,0:T(8,128)(2,1)S(1)}, f32[32,128]{1,0:T(8,128)S(1)}) custom-call(bf16[256,384]{1,0:T(8,128)(2,1)} %x_hbm.1, bf16[3072,128]{1,0:T(8,128)(2,1)} %w_hbm.1, bf16[256,128]{1,0:T(8,128)(2,1)} %v_hbm.1, bf16[256,128]{1,0:T(8,128)(2,1)} %gf_hbm.1, ...), custom_call_target="tpu_custom_call" | custom-call | tf_op jit(solution)/shard_map/pallas_call | solution.py:559
  52.3 0.8 %shard_map.129 = (bf16[256,128]{1,0:T(8,128)(2,1)}, f32[256,128]{1,0:T(8,128)}, f32[256,128]{1,0:T(8,128)}, bf16[256,128]{1,0:T(8,128)(2,1)}, f32[32,128]{1,0:T(8,128)}) custom-call(bf16[256,128]{1,0:T(8,128)(2,1)S(1)} %get-tuple-element.10.refs_0_, f32[256,128]{1,0:T(8,128)S(1)} %get-tuple-element.11.refs_1_, f32[256,128]{1,0:T(8,128)S(1)} %get-tuple-element.12.refs_2_, ...), custom_call_target="tpu_custom_call" | custom-call | tf_op jit(solution)/shard_map/pallas_call | solution.py:595

commit v6 on v5

--- a/solution.py
+++ b/solution.py
@@ -13,7 +13,7 @@
 NZ, NY = 12, 8
 NEAR = 3
 GROUPS = (2, 1)
-EARLY, MIDDLE = 1, 3
+EARLY, MIDDLE, LOW = 1, 3, 2
 EPS = 1e-6
 MESH_ID = pl.DeviceIdType.MESH
 F32, BF16 = jnp.float32, jnp.bfloat16
@@ -165,8 +165,8 @@
     spikes_b = jnp.sum(jnp.where(upper, extra_ref[1], 0.0), axis=1, keepdims=True)
     run = jnp.concatenate(
         [
-            summed(lower_ones, forget[:, :WIDTH], 3) + spikes_f,
-            summed(upper_ones, forget[:, WIDTH:], 3) + spikes_b,
+            summed(lower_ones, forget[:, :WIDTH], 2) + spikes_f,
+            summed(upper_ones, forget[:, WIDTH:], 2) + spikes_b,
         ],
         axis=1,
     )
@@ -413,20 +413,33 @@
 
     fill(0)
     far_send(0)
-    near_fill(range(EARLY))
+    near_fill(range(EARLY + 1))
     near_send(range(EARLY))
+
+    @pl.when(z < LOW)
+    def _():
+        near_send(range(EARLY, EARLY + 1))
+
     fill(1)
     far_send(1)
     fill(2)
     far_send(2)
-    near_fill(range(EARLY, near))
+    near_fill(range(EARLY + 1, near))
 
     decays2 = [swapped(d) for d in decays1]
     lines2 = [swapped(d) for d in lines1]
     arrived("a2", in2.at[others_y], next_y)
     up, down, total_up, total_down = line_fold(in2, decays2)
     second_phase("b2", mid2, got2, (total_up, total_down))
-    near_send(range(EARLY, MIDDLE))
+    @pl.when(z >= LOW)
+    def _():
+        near_send(range(EARLY, EARLY + 1))
+
+    near_send(range(EARLY + 1, MIDDLE))
+
+    @pl.when(z < LOW)
+    def _():
+        near_send(range(MIDDLE, near))
 
     dv = dot(scores, grad_out, TN)
     dk_f = jnp.concatenate(
@@ -448,7 +461,11 @@
     left = jnp.exp(closing) * state.astype(F32) + local
 
     far_pass(0)
-    near_send(range(MIDDLE, near))
+
+    @pl.when(z >= LOW)
+    def _():
+        near_send(range(MIDDLE, near))
+
     arrived("b2", got2.at[others_z], next_z)
     entry = line_entry(got2, lines2)
     third_phase("c2", back2, state2, entry, (up, down), decays2)

time: 53.2 us -> 53.1 us (level)
  the two profiles are of different devices: /device:TPU:128 before, /device:TPU:6 now
where the time goes in v6:
time: 53.1 us; the launch traced here: 52.2 us
  Pallas kernels  51.5 us (97%)
  between operations  0.64 us (1%)
    pallas_call x1, Pallas kernels, on_device(): pl.pallas_call(functools.partial(kernel, nz, ny, nt), out_shape=tuple((pl...  50.7 us

profile of v6, /device:TPU:6, one launch (start us, length us, event | category | flops | bytes accessed | tf_op | source)
XLA Modules:
  0.0 52.2 jit_solution(279771940592632246)
XLA Ops:
  0.6 50.7 %shard_map.128 = (bf16[256,128]{1,0:T(8,128)(2,1)S(1)}, f32[256,128]{1,0:T(8,128)S(1)}, f32[256,128]{1,0:T(8,128)S(1)}, bf16[256,128]{1,0:T(8,128)(2,1)S(1)}, f32[32,128]{1,0:T(8,128)S(1)}) custom-call(bf16[256,384]{1,0:T(8,128)(2,1)} %x_hbm.1, bf16[3072,128]{1,0:T(8,128)(2,1)} %w_hbm.1, bf16[256,128]{1,0:T(8,128)(2,1)} %v_hbm.1, bf16[256,128]{1,0:T(8,128)(2,1)} %gf_hbm.1, ...), custom_call_target="tpu_custom_call" | custom-call | tf_op jit(solution)/shard_map/pallas_call | solution.py:576
  51.4 0.8 %shard_map.129 = (bf16[256,128]{1,0:T(8,128)(2,1)}, f32[256,128]{1,0:T(8,128)}, f32[256,128]{1,0:T(8,128)}, bf16[256,128]{1,0:T(8,128)(2,1)}, f32[32,128]{1,0:T(8,128)}) custom-call(bf16[256,128]{1,0:T(8,128)(2,1)S(1)} %get-tuple-element.10.refs_0_, f32[256,128]{1,0:T(8,128)S(1)} %get-tuple-element.11.refs_1_, f32[256,128]{1,0:T(8,128)S(1)} %get-tuple-element.12.refs_2_, ...), custom_call_target="tpu_custom_call" | custom-call | tf_op jit(solution)/shard_map/pallas_call | solution.py:612

commit v7 on v6

--- a/solution.py
+++ b/solution.py
@@ -470,16 +470,20 @@
     entry = line_entry(got2, lines2)
     third_phase("c2", back2, state2, entry, (up, down), decays2)
 
+    def near_pass():
+        arrived("b3", wb_in, next_z)
+        acc = wb_in[0].astype(F32)
+        for i in range(1, near):
+            acc += wb_in[i].astype(F32)
+        wb_mid[...] = acc.astype(BF16)
+        for o in far_first(ny):
+            k = at_y(o)
+            send("a4", wb_mid.at[k], wb_got.at[y], {"sp_1": k})
+
+    pl.when(z < LOW)(near_pass)
     own = far_pass(1)
     far_pass(2)
-    arrived("b3", wb_in, next_z)
-    acc = wb_in[0].astype(F32)
-    for i in range(1, near):
-        acc += wb_in[i].astype(F32)
-    wb_mid[...] = acc.astype(BF16)
-    for o in far_first(ny):
-        k = at_y(o)
-        send("a4", wb_mid.at[k], wb_got.at[y], {"sp_1": k})
+    pl.when(z >= LOW)(near_pass)
     own += wb_mid[pl.ds(y, 1)].astype(F32).reshape(dw_ref.shape)
 
     arrived("c2", state2.at[pl.ds(0, WIDTH - rows), :], next_y)

time: 53.1 us -> 53.1 us (level)
  the two profiles are of different devices: /device:TPU:6 before, /device:TPU:134 now
where the time goes in v7:
time: 53.1 us; the launch traced here: 52.9 us
  Pallas kernels  52.3 us (98%)
  between operations  0.64 us (1%)
    pallas_call x1, Pallas kernels, on_device(): pl.pallas_call(functools.partial(kernel, nz, ny, nt), out_shape=tuple((pl...  51.5 us

profile of v7, /device:TPU:134, one launch (start us, length us, event | category | flops | bytes accessed | tf_op | source)
XLA Modules:
  0.0 52.9 jit_solution(6261773563714417103)
XLA Ops:
  0.6 51.5 %shard_map.128 = (bf16[256,128]{1,0:T(8,128)(2,1)S(1)}, f32[256,128]{1,0:T(8,128)S(1)}, f32[256,128]{1,0:T(8,128)S(1)}, bf16[256,128]{1,0:T(8,128)(2,1)S(1)}, f32[32,128]{1,0:T(8,128)S(1)}) custom-call(bf16[256,384]{1,0:T(8,128)(2,1)} %x_hbm.1, bf16[3072,128]{1,0:T(8,128)(2,1)} %w_hbm.1, bf16[256,128]{1,0:T(8,128)(2,1)} %v_hbm.1, bf16[256,128]{1,0:T(8,128)(2,1)} %gf_hbm.1, ...), custom_call_target="tpu_custom_call" | custom-call | tf_op jit(solution)/shard_map/pallas_call | solution.py:580
  52.2 0.8 %shard_map.129 = (bf16[256,128]{1,0:T(8,128)(2,1)}, f32[256,128]{1,0:T(8,128)}, f32[256,128]{1,0:T(8,128)}, bf16[256,128]{1,0:T(8,128)(2,1)}, f32[32,128]{1,0:T(8,128)}) custom-call(bf16[256,128]{1,0:T(8,128)(2,1)S(1)} %get-tuple-element.10.refs_0_, f32[256,128]{1,0:T(8,128)S(1)} %get-tuple-element.11.refs_1_, f32[256,128]{1,0:T(8,128)S(1)} %get-tuple-element.12.refs_2_, ...), custom_call_target="tpu_custom_call" | custom-call | tf_op jit(solution)/shard_map/pallas_call | solution.py:616
